TPU v7x, 32 devices: a whole 2x2x4 slice. The times are simulated.
32 devices in a mesh: sp: 8 (over z, y), tp: 4 (over x, core).
Axes of the slice: x: 2, y: 2, z: 4, core: 2. Of those that a mesh axis runs over, the one named last changes fastest.
Arguments:
- tokens: bfloat16 [4096, 4096], P('sp', 'tp'), may hold values from -64 to 64
- norm_gain: float32 [4096], replicated, may hold values from 0.1 to 1.9
- w_query: bfloat16 [4096, 1024], P(None, 'tp'), may hold values from -0.09375 to 0.09375
- w_key: bfloat16 [4096, 1024], P(None, 'tp'), may hold values from -0.09375 to 0.09375
- w_value: bfloat16 [4096, 1024], P(None, 'tp'), may hold values from -0.09375 to 0.09375
- w_gate_out: bfloat16 [4096, 1024], P(None, 'tp'), may hold values from -0.09375 to 0.09375
- w_gate_in: bfloat16 [4096, 1024], P(None, 'tp'), may hold values from -0.09375 to 0.09375
- w_conv_in: bfloat16 [4096, 1024], P(None, 'tp'), may hold values from -0.09375 to 0.09375
- conv_taps: float32 [3, 1024], replicated, may hold values from -3.5 to 3.5
- key_bias: bfloat16 [4096, 16], P('sp', 'tp'), may hold values from -16 to 0
- mix_gain: float32 [2048], replicated, may hold values from 0.1 to 1.9
- out_attn: bfloat16 [1024, 4096], P('tp'), may hold values from -0.125 to 0.125
- out_conv: bfloat16 [1024, 4096], P('tp'), may hold values from -0.125 to 0.125
Outputs:
- mixed: bfloat16 [4096, 4096], P('sp', 'tp')
All inputs are finite; a program needn't handle non-finite values.
Results may differ from a plain program's by a relative error of at most 0.015.
Values may be sent and summed in bfloat16 or wider, within the bound.
A program may use at most 128 MiB of HBM per device.

v0:
```python
import math

import jax
import jax.numpy as jnp
from jax import lax
from jax.sharding import PartitionSpec as P

HEAD = 64
STICK_HEADS = 16
CONV_WIDTH = 3


eps = 1e-06


def from_behind(shard, axis, by):
    count = lax.axis_size(axis)
    pairs = [(i, i + by) for i in range(count) if 0 <= i + by < count]
    return lax.ppermute(shard, axis, pairs)


def stick_terms(queries, key_rows, value_rows, bias_rows, survival, causal):
    tok_rows, head_count, head_width = queries.shape
    key_count = key_rows.shape[0]
    key_span = math.gcd(key_count, 128)
    blocks = key_count // key_span
    key_heads = key_rows.reshape(key_count, head_count, head_width)
    value_heads = value_rows.reshape(key_count, head_count, head_width)
    scores = jnp.einsum("qhe,khe->hqk", queries, key_heads, preferred_element_type=jnp.float32)
    scores = (
        scores * head_width ** (-0.5) + jnp.transpose(bias_rows.astype(jnp.float32))[:, None, :]
    )
    log_rest = jax.nn.log_sigmoid(-scores)
    log_take = jax.nn.log_sigmoid(scores)
    earlier = jnp.arange(key_count)[None, :] < jnp.arange(tok_rows)[:, None]
    if causal:
        log_rest = jnp.where(earlier[None], log_rest, 0.0)
    pieces = log_rest.reshape(head_count, tok_rows, blocks, key_span)
    inner = jnp.arange(key_span)
    after_mat = (inner[:, None] > inner[None, :]).astype(jnp.float32)
    within = jnp.einsum("hqbj,js->hqbs", pieces, after_mat, precision=lax.Precision.HIGHEST)
    totals = jnp.sum(pieces, axis=-1)
    outer = jnp.arange(blocks)
    later_mat = (outer[:, None] > outer[None, :]).astype(jnp.float32)
    later_sum = jnp.einsum("hqb,bc->hqc", totals, later_mat, precision=lax.Precision.HIGHEST)
    after_sum = within + later_sum[..., None] + survival[:, :, None, None]
    weights = jnp.exp(log_take + after_sum.reshape(head_count, tok_rows, key_count))
    if causal:
        weights = jnp.where(earlier[None], weights, 0.0)
    weights = weights.astype(jnp.bfloat16)
    result = jnp.einsum("hqk,khe->qhe", weights, value_heads, preferred_element_type=jnp.float32)
    return (result, survival + jnp.sum(totals, axis=-1))


def group_norm(value_matrix, gain):
    tok_rows = value_matrix.shape[0]
    grouped = value_matrix.reshape(tok_rows, -1, HEAD)
    grouped = grouped * lax.rsqrt(jnp.mean(grouped * grouped, axis=-1, keepdims=True) + eps)
    return grouped.reshape(tok_rows, -1) * gain


def per_device(
    tokens,
    norm_gain,
    w_query,
    w_key,
    w_value,
    w_gate_out,
    w_gate_in,
    w_conv_in,
    conv_taps,
    key_bias,
    mix_gain,
    out_attn,
    out_conv,
):
    tok_rows = tokens.shape[0]
    head_cols = w_query.shape[1]
    head_count = head_cols // HEAD
    chan_count = w_conv_in.shape[1]
    tp_index = lax.axis_index("tp")
    own_index = lax.axis_index("sp")
    sp_count = lax.axis_size("sp")
    weights = jnp.concatenate([w_query, w_key, w_value, w_gate_out, w_gate_in, w_conv_in], axis=1)
    gathered = lax.all_gather(tokens, "tp", axis=1, tiled=True)
    tok_float = gathered.astype(jnp.float32)
    row_scale = lax.rsqrt(jnp.mean(tok_float * tok_float, axis=1, keepdims=True) + eps)
    normed = (tok_float * row_scale * norm_gain).astype(jnp.bfloat16)
    projected = jnp.dot(normed, weights, preferred_element_type=jnp.float32)
    projected = projected.astype(jnp.bfloat16)
    queries = projected[:, :head_cols].reshape(tok_rows, head_count, HEAD)
    key_rows = projected[:, head_cols : 2 * head_cols]
    value_rows = projected[:, 2 * head_cols : 3 * head_cols]
    conv_base = 3 * head_cols
    gate_out = projected[:, conv_base : conv_base + chan_count]
    gate_in = projected[:, conv_base + chan_count : conv_base + 2 * chan_count]
    conv_in = projected[:, conv_base + 2 * chan_count : conv_base + 3 * chan_count]
    edge_rows = CONV_WIDTH - 1
    tail_rows = jnp.stack([gate_in[tok_rows - edge_rows :], conv_in[tok_rows - edge_rows :]])
    before = from_behind(tail_rows, "sp", 1)
    zero_state = jnp.zeros((head_count, tok_rows), jnp.float32)
    result, survival = stick_terms(queries, key_rows, value_rows, key_bias, zero_state, True)

    def further(offset, loop_state):
        running, carried, held_keys = loop_state
        held_keys = from_behind((held_keys[0], held_keys[1], held_keys[2]), "sp", 1)

        def take_keys(pair_state):
            added, moved = stick_terms(
                queries, held_keys[0], held_keys[1], held_keys[2], pair_state[1], False
            )
            return (pair_state[0] + added, moved)

        def keep_state(pair_state):
            return pair_state

        running, carried = lax.cond(own_index >= offset, take_keys, keep_state, (running, carried))
        return (running, carried, held_keys)

    result, survival, held_last = lax.fori_loop(
        1, sp_count, further, (result, survival, (key_rows, value_rows, key_bias))
    )
    mixed_in = gate_in.astype(jnp.float32) * conv_in.astype(jnp.float32)
    earlier_mixed = before[0].astype(jnp.float32) * before[1].astype(jnp.float32)
    padded = jnp.concatenate([earlier_mixed, mixed_in], axis=0)
    own_taps = lax.dynamic_slice_in_dim(conv_taps, tp_index * chan_count, chan_count, 1)
    convolved = jnp.zeros((tok_rows, chan_count), jnp.float32)
    for tap_index in range(CONV_WIDTH):
        convolved = convolved + own_taps[tap_index] * padded[tap_index : tap_index + tok_rows]
    conv_out = gate_out.astype(jnp.float32) * convolved
    attn_gain = lax.dynamic_slice_in_dim(mix_gain, tp_index * head_cols, head_cols)
    conv_gain = lax.dynamic_slice_in_dim(
        mix_gain, STICK_HEADS * HEAD + tp_index * chan_count, chan_count
    )
    attn_normed = group_norm(result.reshape(tok_rows, head_cols), attn_gain).astype(jnp.bfloat16)
    conv_normed = group_norm(conv_out, conv_gain).astype(jnp.bfloat16)
    out_terms = jnp.dot(attn_normed, out_attn, preferred_element_type=jnp.float32)
    out_terms = out_terms + jnp.dot(conv_normed, out_conv, preferred_element_type=jnp.float32)
    return lax.psum_scatter(out_terms.astype(jnp.bfloat16), "tp", scatter_dimension=1, tiled=True)


def solution(mesh):
    in_specs = (
        P("sp", "tp"),
        P(),
        P(None, "tp"),
        P(None, "tp"),
        P(None, "tp"),
        P(None, "tp"),
        P(None, "tp"),
        P(None, "tp"),
        P(),
        P("sp", "tp"),
        P(),
        P("tp", None),
        P("tp", None),
    )
    out_specs = P("sp", "tp")
    return jax.shard_map(
        per_device, mesh=mesh, in_specs=in_specs, out_specs=out_specs, check_vma=False
    )
```

profile of v0, /device:TPU:29, one launch (start us, length us, event | category | flops | bytes accessed | tf_op | source)
XLA Modules:
  0.0 357.6 jit_solution(11451394257962057576)
XLA Ops:
  9.4 3.3 constant_dynamic-update-slice_fusion.5
  12.7 1.7 constant_dynamic-update-slice_fusion.4
  14.4 1.7 constant_dynamic-update-slice_fusion.3
  16.1 1.6 constant_dynamic-update-slice_fusion.2
  17.7 1.7 constant_dynamic-update-slice_fusion.1
  19.4 1.6 constant_dynamic-update-slice_fusion
  21.0 23.7 %all-gather.2.cloned.1.call-done = bf16[512,4096]{1,0:T(8,128)(2,1)} async-done(((bf16[512,1024]{1,0:T(8,128)(2,1)}), bf16[512,4096]{1,0:T(8,128)(2,1)}) %all-gather.2.cloned.1.call-update) | async-done | bytes 4194320 | tf_op jit(solution)/shard_map/all_gather | solution.py:85
  44.7 3.2 fusion.13
  48.2 9.8 %fusion.25 = bf16[512,1536]{1,0:T(8,128)(2,1)S(1)} fusion(bf16[4096,1536]{1,0:T(8,128)(2,1)} %constant_dynamic-update-slice_fusion, bf16[512,4096]{1,0:T(8,128)(2,1)S(1)} %copy-done.1, f32[4096]{0:T(1024)S(1)} %copy-done.9, f32[512]{0:T(512)S(1)} %add_rsqrt_fusion.2), kind=kOutput, calls=%fused_computation.42 | convolution fusion | flops 6451625984 | bytes 18368512 | tf_op jit(solution)/shard_map/dot_general | solution.py:89
  61.1 2.2 fusion.28
  63.3 3.3 fusion.45
  67.3 2.9 convolution_add_fusion
  70.2 3.9 %fusion.22 = bf16[4,512,512]{1,2,0:T(8,128)(2,1)S(1)} fusion(f32[4,512,4,128]{1,3,2,0:T(8,128)S(1)} %convolution_add_fusion, f32[4,512,512]{1,2,0:T(8,128)S(1)} %get-tuple-element.226, f32[4,512]{1,0:T(4,128)S(1)} %convert_bitcast_fusion.1, pred[512,512]{0,1:T(8,128)(4,1)S(1)} %iota_compare_fusion.2), kind=kLoop, calls=%fused_computation.35 | loop fusion | flops 13631488 | bytes 10756096 | tf_op jit(solution)/shard_map/convert_element_type | solution.py:50
  74.6 206.9 %while.21 = (s32[]{:T(128)}, f32[512,4,64]{0,2,1:T(8,128)S(1)}, f32[4,512]{1,0:T(4,128)S(1)}, bf16[512,256]{0,1:T(8,128)(2,1)}, bf16[512,256]{0,1:T(8,128)(2,1)S...) while((s32[]{:T(128)}, f32[512,4,64]{0,2,1:T(8,128)S(1)}, ...), condition=%wide.region_8.9_spmd, body=%wide.region_3.8_spmd.sunk | while | flops 1925459968 | bytes 39555384 | solution.py:120
  74.8 1.3 collective-permute-start
  76.1 1.3 collective-permute-start.2
  77.4 1.3 collective-permute-start.1
  78.7 11.5 %collective-permute-done.1 = bf16[512,4]{0,1:T(4,128)(2,1)S(1)} collective-permute-done((bf16[512,4]{0,1:T(4,128)(2,1)S(1)}, bf16[512,4]{0,1:T(4,128)(2,1)S(1)}, u32[]{:S(2)}, u32[]{:S(2)}) %collective-permute-start.1) | collective-permute-done | bytes 4128 | tf_op jit(solution)/shard_map/while/body/eval_jaxpr/ppermute | solution.py:19
  90.2 15.3 %conditional.2 = ((f32[512,4,64]{0,2,1:T(8,128)S(1)}, f32[4,512]{1,0:T(4,128)S(1)})) conditional(s32[]{:T(128)} %convert_element_type.95, (f32[512,4,64]{0,2,1:T(8,128)S(1)}, f32[4,512]{1,0:T(4,128)S(1)}) %tuple.51, (bf16[512,256]{0,1:T(8,128)(2,1)S(1)}, bf16[512,4,64]{0,2,1:T(8,128)(2,1)}, bf16[512,4]{0,1:T(4,128)(2,1)S(1)}, f32[4,512]{1,0:T(4,128)S(1)}, ...), branch_computations={%region_4.4_spmd, %region_5.7_spmd} | conditional | flops 1925459968 | bytes 36384792 | solution.py:117
  90.3 2.1 fusion.7
  92.4 3.2 bitcast_reduce_fusion
  95.7 3.1 add_add_fusion
  98.8 6.2 %fusion.4 = (f32[4,512]{1,0:T(4,128)S(1)}, bf16[4,512,512]{1,2,0:T(8,128)(2,1)S(1)}) fusion(f32[4,512]{1,0:T(4,128)S(1)} %convert_bitcast_fusion, f32[4,512,512]{1,2,0:T(8,128)S(1)} %get-tuple-element.214, u8[512,512]{0,1:T(8,128)(4,1)S(1)} %get-tuple-element.213, f32[4,512,4,128]{1,3,2,0:T(8,128)S(1)} %add_add_fusion), kind=kLoop, calls=%fused_computation.10 | loop fusion | flops 23066624 | bytes 10764288 | tf_op jit(solution)/shard_map/while/body/eval_jaxpr/cond/branch_1_fun/reduce_sum | solution.py:52
  106.3 1.3 collective-permute-start
  110.2 10.6 %collective-permute-done.1 = bf16[512,4]{0,1:T(4,128)(2,1)S(1)} collective-permute-done((bf16[512,4]{0,1:T(4,128)(2,1)S(1)}, bf16[512,4]{0,1:T(4,128)(2,1)S(1)}, u32[]{:S(2)}, u32[]{:S(2)}) %collective-permute-start.1) | collective-permute-done | bytes 4128 | tf_op jit(solution)/shard_map/while/body/eval_jaxpr/ppermute | solution.py:19
  120.9 15.3 %conditional.2 = ((f32[512,4,64]{0,2,1:T(8,128)S(1)}, f32[4,512]{1,0:T(4,128)S(1)})) conditional(s32[]{:T(128)} %convert_element_type.95, (f32[512,4,64]{0,2,1:T(8,128)S(1)}, f32[4,512]{1,0:T(4,128)S(1)}) %tuple.51, (bf16[512,256]{0,1:T(8,128)(2,1)S(1)}, bf16[512,4,64]{0,2,1:T(8,128)(2,1)}, bf16[512,4]{0,1:T(4,128)(2,1)S(1)}, f32[4,512]{1,0:T(4,128)S(1)}, ...), branch_computations={%region_4.4_spmd, %region_5.7_spmd} | conditional | flops 1925459968 | bytes 36384792 | solution.py:117
  120.9 2.1 fusion.7
  123.0 3.2 bitcast_reduce_fusion
  126.4 3.1 add_add_fusion
  129.4 6.2 %fusion.4 = (f32[4,512]{1,0:T(4,128)S(1)}, bf16[4,512,512]{1,2,0:T(8,128)(2,1)S(1)}) fusion(f32[4,512]{1,0:T(4,128)S(1)} %convert_bitcast_fusion, f32[4,512,512]{1,2,0:T(8,128)S(1)} %get-tuple-element.214, u8[512,512]{0,1:T(8,128)(4,1)S(1)} %get-tuple-element.213, f32[4,512,4,128]{1,3,2,0:T(8,128)S(1)} %add_add_fusion), kind=kLoop, calls=%fused_computation.10 | loop fusion | flops 23066624 | bytes 10764288 | tf_op jit(solution)/shard_map/while/body/eval_jaxpr/cond/branch_1_fun/reduce_sum | solution.py:52
  140.9 10.6 %collective-permute-done.1 = bf16[512,4]{0,1:T(4,128)(2,1)S(1)} collective-permute-done((bf16[512,4]{0,1:T(4,128)(2,1)S(1)}, bf16[512,4]{0,1:T(4,128)(2,1)S(1)}, u32[]{:S(2)}, u32[]{:S(2)}) %collective-permute-start.1) | collective-permute-done | bytes 4128 | tf_op jit(solution)/shard_map/while/body/eval_jaxpr/ppermute | solution.py:19
  151.5 15.3 %conditional.2 = ((f32[512,4,64]{0,2,1:T(8,128)S(1)}, f32[4,512]{1,0:T(4,128)S(1)})) conditional(s32[]{:T(128)} %convert_element_type.95, (f32[512,4,64]{0,2,1:T(8,128)S(1)}, f32[4,512]{1,0:T(4,128)S(1)}) %tuple.51, (bf16[512,256]{0,1:T(8,128)(2,1)S(1)}, bf16[512,4,64]{0,2,1:T(8,128)(2,1)}, bf16[512,4]{0,1:T(4,128)(2,1)S(1)}, f32[4,512]{1,0:T(4,128)S(1)}, ...), branch_computations={%region_4.4_spmd, %region_5.7_spmd} | conditional | flops 1925459968 | bytes 36384792 | solution.py:117
  151.5 2.1 fusion.7
  153.7 3.2 bitcast_reduce_fusion
  157.0 3.1 add_add_fusion
  160.1 6.2 %fusion.4 = (f32[4,512]{1,0:T(4,128)S(1)}, bf16[4,512,512]{1,2,0:T(8,128)(2,1)S(1)}) fusion(f32[4,512]{1,0:T(4,128)S(1)} %convert_bitcast_fusion, f32[4,512,512]{1,2,0:T(8,128)S(1)} %get-tuple-element.214, u8[512,512]{0,1:T(8,128)(4,1)S(1)} %get-tuple-element.213, f32[4,512,4,128]{1,3,2,0:T(8,128)S(1)} %add_add_fusion), kind=kLoop, calls=%fused_computation.10 | loop fusion | flops 23066624 | bytes 10764288 | tf_op jit(solution)/shard_map/while/body/eval_jaxpr/cond/branch_1_fun/reduce_sum | solution.py:52
  171.5 9.8 %collective-permute-done.1 = bf16[512,4]{0,1:T(4,128)(2,1)S(1)} collective-permute-done((bf16[512,4]{0,1:T(4,128)(2,1)S(1)}, bf16[512,4]{0,1:T(4,128)(2,1)S(1)}, u32[]{:S(2)}, u32[]{:S(2)}) %collective-permute-start.1) | collective-permute-done | bytes 4128 | tf_op jit(solution)/shard_map/while/body/eval_jaxpr/ppermute | solution.py:19
  181.3 15.3 %conditional.2 = ((f32[512,4,64]{0,2,1:T(8,128)S(1)}, f32[4,512]{1,0:T(4,128)S(1)})) conditional(s32[]{:T(128)} %convert_element_type.95, (f32[512,4,64]{0,2,1:T(8,128)S(1)}, f32[4,512]{1,0:T(4,128)S(1)}) %tuple.51, (bf16[512,256]{0,1:T(8,128)(2,1)S(1)}, bf16[512,4,64]{0,2,1:T(8,128)(2,1)}, bf16[512,4]{0,1:T(4,128)(2,1)S(1)}, f32[4,512]{1,0:T(4,128)S(1)}, ...), branch_computations={%region_4.4_spmd, %region_5.7_spmd} | conditional | flops 1925459968 | bytes 36384792 | solution.py:117
  181.3 2.1 fusion.7
  183.4 3.2 bitcast_reduce_fusion
  186.8 3.1 add_add_fusion
  189.8 6.2 %fusion.4 = (f32[4,512]{1,0:T(4,128)S(1)}, bf16[4,512,512]{1,2,0:T(8,128)(2,1)S(1)}) fusion(f32[4,512]{1,0:T(4,128)S(1)} %convert_bitcast_fusion, f32[4,512,512]{1,2,0:T(8,128)S(1)} %get-tuple-element.214, u8[512,512]{0,1:T(8,128)(4,1)S(1)} %get-tuple-element.213, f32[4,512,4,128]{1,3,2,0:T(8,128)S(1)} %add_add_fusion), kind=kLoop, calls=%fused_computation.10 | loop fusion | flops 23066624 | bytes 10764288 | tf_op jit(solution)/shard_map/while/body/eval_jaxpr/cond/branch_1_fun/reduce_sum | solution.py:52
  201.2 8.9 %collective-permute-done.1 = bf16[512,4]{0,1:T(4,128)(2,1)S(1)} collective-permute-done((bf16[512,4]{0,1:T(4,128)(2,1)S(1)}, bf16[512,4]{0,1:T(4,128)(2,1)S(1)}, u32[]{:S(2)}, u32[]{:S(2)}) %collective-permute-start.1) | collective-permute-done | bytes 4128 | tf_op jit(solution)/shard_map/while/body/eval_jaxpr/ppermute | solution.py:19
  210.2 15.3 %conditional.2 = ((f32[512,4,64]{0,2,1:T(8,128)S(1)}, f32[4,512]{1,0:T(4,128)S(1)})) conditional(s32[]{:T(128)} %convert_element_type.95, (f32[512,4,64]{0,2,1:T(8,128)S(1)}, f32[4,512]{1,0:T(4,128)S(1)}) %tuple.51, (bf16[512,256]{0,1:T(8,128)(2,1)S(1)}, bf16[512,4,64]{0,2,1:T(8,128)(2,1)}, bf16[512,4]{0,1:T(4,128)(2,1)S(1)}, f32[4,512]{1,0:T(4,128)S(1)}, ...), branch_computations={%region_4.4_spmd, %region_5.7_spmd} | conditional | flops 1925459968 | bytes 36384792 | solution.py:117
  210.2 2.1 fusion.7
  212.3 3.2 bitcast_reduce_fusion
  215.7 3.1 add_add_fusion
  218.7 6.2 %fusion.4 = (f32[4,512]{1,0:T(4,128)S(1)}, bf16[4,512,512]{1,2,0:T(8,128)(2,1)S(1)}) fusion(f32[4,512]{1,0:T(4,128)S(1)} %convert_bitcast_fusion, f32[4,512,512]{1,2,0:T(8,128)S(1)} %get-tuple-element.214, u8[512,512]{0,1:T(8,128)(4,1)S(1)} %get-tuple-element.213, f32[4,512,4,128]{1,3,2,0:T(8,128)S(1)} %add_add_fusion), kind=kLoop, calls=%fused_computation.10 | loop fusion | flops 23066624 | bytes 10764288 | tf_op jit(solution)/shard_map/while/body/eval_jaxpr/cond/branch_1_fun/reduce_sum | solution.py:52
  230.2 8.0 %collective-permute-done.1 = bf16[512,4]{0,1:T(4,128)(2,1)S(1)} collective-permute-done((bf16[512,4]{0,1:T(4,128)(2,1)S(1)}, bf16[512,4]{0,1:T(4,128)(2,1)S(1)}, u32[]{:S(2)}, u32[]{:S(2)}) %collective-permute-start.1) | collective-permute-done | bytes 4128 | tf_op jit(solution)/shard_map/while/body/eval_jaxpr/ppermute | solution.py:19
  238.2 15.3 %conditional.2 = ((f32[512,4,64]{0,2,1:T(8,128)S(1)}, f32[4,512]{1,0:T(4,128)S(1)})) conditional(s32[]{:T(128)} %convert_element_type.95, (f32[512,4,64]{0,2,1:T(8,128)S(1)}, f32[4,512]{1,0:T(4,128)S(1)}) %tuple.51, (bf16[512,256]{0,1:T(8,128)(2,1)S(1)}, bf16[512,4,64]{0,2,1:T(8,128)(2,1)}, bf16[512,4]{0,1:T(4,128)(2,1)S(1)}, f32[4,512]{1,0:T(4,128)S(1)}, ...), branch_computations={%region_4.4_spmd, %region_5.7_spmd} | conditional | flops 1925459968 | bytes 36384792 | solution.py:117
  238.2 2.1 fusion.7
  240.4 3.2 bitcast_reduce_fusion
  243.7 3.1 add_add_fusion
  246.8 6.2 %fusion.4 = (f32[4,512]{1,0:T(4,128)S(1)}, bf16[4,512,512]{1,2,0:T(8,128)(2,1)S(1)}) fusion(f32[4,512]{1,0:T(4,128)S(1)} %convert_bitcast_fusion, f32[4,512,512]{1,2,0:T(8,128)S(1)} %get-tuple-element.214, u8[512,512]{0,1:T(8,128)(4,1)S(1)} %get-tuple-element.213, f32[4,512,4,128]{1,3,2,0:T(8,128)S(1)} %add_add_fusion), kind=kLoop, calls=%fused_computation.10 | loop fusion | flops 23066624 | bytes 10764288 | tf_op jit(solution)/shard_map/while/body/eval_jaxpr/cond/branch_1_fun/reduce_sum | solution.py:52
  258.2 7.2 %collective-permute-done.1 = bf16[512,4]{0,1:T(4,128)(2,1)S(1)} collective-permute-done((bf16[512,4]{0,1:T(4,128)(2,1)S(1)}, bf16[512,4]{0,1:T(4,128)(2,1)S(1)}, u32[]{:S(2)}, u32[]{:S(2)}) %collective-permute-start.1) | collective-permute-done | bytes 4128 | tf_op jit(solution)/shard_map/while/body/eval_jaxpr/ppermute | solution.py:19
  265.4 15.3 %conditional.2 = ((f32[512,4,64]{0,2,1:T(8,128)S(1)}, f32[4,512]{1,0:T(4,128)S(1)})) conditional(s32[]{:T(128)} %convert_element_type.95, (f32[512,4,64]{0,2,1:T(8,128)S(1)}, f32[4,512]{1,0:T(4,128)S(1)}) %tuple.51, (bf16[512,256]{0,1:T(8,128)(2,1)S(1)}, bf16[512,4,64]{0,2,1:T(8,128)(2,1)}, bf16[512,4]{0,1:T(4,128)(2,1)S(1)}, f32[4,512]{1,0:T(4,128)S(1)}, ...), branch_computations={%region_4.4_spmd, %region_5.7_spmd} | conditional | flops 1925459968 | bytes 36384792 | solution.py:117
  265.5 2.1 fusion.7
  267.6 3.2 bitcast_reduce_fusion
  270.9 3.1 add_add_fusion
  274.0 6.2 %fusion.4 = (f32[4,512]{1,0:T(4,128)S(1)}, bf16[4,512,512]{1,2,0:T(8,128)(2,1)S(1)}) fusion(f32[4,512]{1,0:T(4,128)S(1)} %convert_bitcast_fusion, f32[4,512,512]{1,2,0:T(8,128)S(1)} %get-tuple-element.214, u8[512,512]{0,1:T(8,128)(4,1)S(1)} %get-tuple-element.213, f32[4,512,4,128]{1,3,2,0:T(8,128)S(1)} %add_add_fusion), kind=kLoop, calls=%fused_computation.10 | loop fusion | flops 23066624 | bytes 10764288 | tf_op jit(solution)/shard_map/while/body/eval_jaxpr/cond/branch_1_fun/reduce_sum | solution.py:52
  281.7 1.6 collective-permute-start.3
  283.4 4.5 %fusion.48 = f32[512,4096]{1,0:T(8,128)} fusion(bf16[512,256]{0,1:T(8,128)(2,1)S(1)} %fusion.35, bf16[256,4096]{1,0:T(8,128)(2,1)S(1)} %copy-done), kind=kOutput, calls=%fused_computation.89 | convolution fusion | flops 1073741824 | bytes 10747904 | tf_op jit(solution)/shard_map/dot_general | solution.py:137
  292.4 7.2 %add_convert_fusion = bf16[512,4096]{1,0:T(8,128)(2,1)} fusion(f32[512,4096]{1,0:T(8,128)} %fusion.48, bf16[256,4096]{1,0:T(8,128)(2,1)} %param.29, f32[512,256]{1,0:T(8,128)S(1)} %get-tuple-element.208, f32[512,256]{1,0:T(8,128)S(1)} %copy.35, f32[256]{0:T(256)S(1)} %get-tuple-element.223), kind=kOutput, calls=%fused_computation.29 | convolution fusion | flops 1078329344 | bytes 15729664 | tf_op jit(solution)/shard_map/dot_general | solution.py:138
  299.6 51.2 %reduce-scatter.2.cloned.1.call-done = bf16[512,1024]{1,0:T(8,128)(2,1)} async-done(((bf16[512,4096]{1,0:T(8,128)(2,1)}), bf16[512,1024]{1,0:T(8,128)(2,1)}) %reduce-scatter.2.cloned.1.call-update) | async-done | bytes 1048592 | tf_op jit(solution)/shard_map/reduce_scatter | solution.py:139
  (132 shorter events, 43.7 us)
Async XLA Ops:
  6.5 276.8 %copy-start = (bf16[256,4096]{1,0:T(8,128)(2,1)S(1)}, bf16[256,4096]{1,0:T(8,128)(2,1)}, u32[]{:S(2)}) copy-start(bf16[256,4096]{1,0:T(8,128)(2,1)} %param.28) | copy-start | bytes 6291460
  6.5 38.2 %all-gather.2.cloned.1.call-start = ((), (), s32[]{:S(2)}) async-start(), calls=%async_computation.1 | async-start | bytes 5242880 | tf_op jit(solution)/shard_map/all_gather | solution.py:85
  7.4 343.4 %reduce-scatter.2.cloned.1.call-start = ((), (), s32[]{:S(2)}) async-start(), calls=%async_computation.2 | async-start | bytes 5242880 | tf_op jit(solution)/shard_map/reduce_scatter | solution.py:139
  7.5 5.3 %copy-start.2 = (bf16[4096,256]{1,0:T(8,128)(2,1)S(1)}, bf16[4096,256]{1,0:T(8,128)(2,1)}, u32[]{:S(2)}) copy-start(bf16[4096,256]{1,0:T(8,128)(2,1)} %param.20) | copy-start | bytes 6291460
  9.4 5.0 %copy-start.3 = (bf16[4096,256]{1,0:T(8,128)(2,1)S(1)}, bf16[4096,256]{1,0:T(8,128)(2,1)}, u32[]{:S(2)}) copy-start(bf16[4096,256]{1,0:T(8,128)(2,1)} %param.21) | copy-start | bytes 6291460
  12.7 3.4 copy-start.4
  14.4 3.3 copy-start.5
  16.1 3.3 copy-start.6
  19.4 28.6 %copy-start.9 = (f32[4096]{0:T(1024)S(1)}, f32[4096]{0:T(1024)}, u32[]{:S(2)}) copy-start(f32[4096]{0:T(1024)} %param.18) | copy-start | bytes 49156
  44.7 3.4 copy-start.1
  58.0 1.2 copy-start.7
  74.8 15.4 %collective-permute-start = (bf16[512,256]{0,1:T(8,128)(2,1)}, bf16[512,256]{0,1:T(8,128)(2,1)S(1)}, u32[]{:S(2)}, u32[]{:S(2)}) collective-permute-start(bf16[512,256]{0,1:T(8,128)(2,1)} %get-tuple-element.296), channel_id=1, source_target_pairs={{0,4},{4,8},{8,12},{12,16},{16,20},{20,24},{24,28},{1,5},{5,9},{9,... | collective-permute-start | bytes 786440 | tf_op jit(solution)/shard_map/while/body/eval_jaxpr/ppermute | solution.py:19
  76.1 14.1 %collective-permute-start.2 = (bf16[512,256]{0,1:T(8,128)(2,1)S(1)}, bf16[512,256]{0,1:T(8,128)(2,1)S(1)}, u32[]{:S(2)}, u32[]{:S(2)}) collective-permute-start(bf16[512,256]{0,1:T(8,128)(2,1)S(1)} %get-tuple-element.297), channel_id=1, source_target_pairs={{0,4},{4,8},{8,12},{12,16},{16,20},{20,24},{24,28},{1,5},{5,9},{9,... | collective-permute-start | bytes 786440 | tf_op jit(solution)/shard_map/while/body/eval_jaxpr/ppermute | solution.py:19
  77.4 12.8 %collective-permute-start.1 = (bf16[512,4]{0,1:T(4,128)(2,1)S(1)}, bf16[512,4]{0,1:T(4,128)(2,1)S(1)}, u32[]{:S(2)}, u32[]{:S(2)}) collective-permute-start(bf16[512,4]{0,1:T(4,128)(2,1)S(1)} %get-tuple-element.298), channel_id=1, source_target_pairs={{0,4},{4,8},{8,12},{12,16},{16,20},{20,24},{24,28},{1,5},{5,9},{9,... | collective-permute-start | bytes 12296 | tf_op jit(solution)/shard_map/while/body/eval_jaxpr/ppermute | solution.py:19
  106.3 14.6 %collective-permute-start = (bf16[512,256]{0,1:T(8,128)(2,1)}, bf16[512,256]{0,1:T(8,128)(2,1)S(1)}, u32[]{:S(2)}, u32[]{:S(2)}) collective-permute-start(bf16[512,256]{0,1:T(8,128)(2,1)} %get-tuple-element.296), channel_id=1, source_target_pairs={{0,4},{4,8},{8,12},{12,16},{16,20},{20,24},{24,28},{1,5},{5,9},{9,... | collective-permute-start | bytes 786440 | tf_op jit(solution)/shard_map/while/body/eval_jaxpr/ppermute | solution.py:19
  107.6 13.3 %collective-permute-start.2 = (bf16[512,256]{0,1:T(8,128)(2,1)S(1)}, bf16[512,256]{0,1:T(8,128)(2,1)S(1)}, u32[]{:S(2)}, u32[]{:S(2)}) collective-permute-start(bf16[512,256]{0,1:T(8,128)(2,1)S(1)} %get-tuple-element.297), channel_id=1, source_target_pairs={{0,4},{4,8},{8,12},{12,16},{16,20},{20,24},{24,28},{1,5},{5,9},{9,... | collective-permute-start | bytes 786440 | tf_op jit(solution)/shard_map/while/body/eval_jaxpr/ppermute | solution.py:19
  108.9 11.9 %collective-permute-start.1 = (bf16[512,4]{0,1:T(4,128)(2,1)S(1)}, bf16[512,4]{0,1:T(4,128)(2,1)S(1)}, u32[]{:S(2)}, u32[]{:S(2)}) collective-permute-start(bf16[512,4]{0,1:T(4,128)(2,1)S(1)} %get-tuple-element.298), channel_id=1, source_target_pairs={{0,4},{4,8},{8,12},{12,16},{16,20},{20,24},{24,28},{1,5},{5,9},{9,... | collective-permute-start | bytes 12296 | tf_op jit(solution)/shard_map/while/body/eval_jaxpr/ppermute | solution.py:19
  137.0 14.5 %collective-permute-start = (bf16[512,256]{0,1:T(8,128)(2,1)}, bf16[512,256]{0,1:T(8,128)(2,1)S(1)}, u32[]{:S(2)}, u32[]{:S(2)}) collective-permute-start(bf16[512,256]{0,1:T(8,128)(2,1)} %get-tuple-element.296), channel_id=1, source_target_pairs={{0,4},{4,8},{8,12},{12,16},{16,20},{20,24},{24,28},{1,5},{5,9},{9,... | collective-permute-start | bytes 786440 | tf_op jit(solution)/shard_map/while/body/eval_jaxpr/ppermute | solution.py:19
  138.3 13.2 %collective-permute-start.2 = (bf16[512,256]{0,1:T(8,128)(2,1)S(1)}, bf16[512,256]{0,1:T(8,128)(2,1)S(1)}, u32[]{:S(2)}, u32[]{:S(2)}) collective-permute-start(bf16[512,256]{0,1:T(8,128)(2,1)S(1)} %get-tuple-element.297), channel_id=1, source_target_pairs={{0,4},{4,8},{8,12},{12,16},{16,20},{20,24},{24,28},{1,5},{5,9},{9,... | collective-permute-start | bytes 786440 | tf_op jit(solution)/shard_map/while/body/eval_jaxpr/ppermute | solution.py:19
  139.6 11.9 %collective-permute-start.1 = (bf16[512,4]{0,1:T(4,128)(2,1)S(1)}, bf16[512,4]{0,1:T(4,128)(2,1)S(1)}, u32[]{:S(2)}, u32[]{:S(2)}) collective-permute-start(bf16[512,4]{0,1:T(4,128)(2,1)S(1)} %get-tuple-element.298), channel_id=1, source_target_pairs={{0,4},{4,8},{8,12},{12,16},{16,20},{20,24},{24,28},{1,5},{5,9},{9,... | collective-permute-start | bytes 12296 | tf_op jit(solution)/shard_map/while/body/eval_jaxpr/ppermute | solution.py:19
  167.6 13.7 %collective-permute-start = (bf16[512,256]{0,1:T(8,128)(2,1)}, bf16[512,256]{0,1:T(8,128)(2,1)S(1)}, u32[]{:S(2)}, u32[]{:S(2)}) collective-permute-start(bf16[512,256]{0,1:T(8,128)(2,1)} %get-tuple-element.296), channel_id=1, source_target_pairs={{0,4},{4,8},{8,12},{12,16},{16,20},{20,24},{24,28},{1,5},{5,9},{9,... | collective-permute-start | bytes 786440 | tf_op jit(solution)/shard_map/while/body/eval_jaxpr/ppermute | solution.py:19
  168.9 12.4 %collective-permute-start.2 = (bf16[512,256]{0,1:T(8,128)(2,1)S(1)}, bf16[512,256]{0,1:T(8,128)(2,1)S(1)}, u32[]{:S(2)}, u32[]{:S(2)}) collective-permute-start(bf16[512,256]{0,1:T(8,128)(2,1)S(1)} %get-tuple-element.297), channel_id=1, source_target_pairs={{0,4},{4,8},{8,12},{12,16},{16,20},{20,24},{24,28},{1,5},{5,9},{9,... | collective-permute-start | bytes 786440 | tf_op jit(solution)/shard_map/while/body/eval_jaxpr/ppermute | solution.py:19
  170.2 11.1 %collective-permute-start.1 = (bf16[512,4]{0,1:T(4,128)(2,1)S(1)}, bf16[512,4]{0,1:T(4,128)(2,1)S(1)}, u32[]{:S(2)}, u32[]{:S(2)}) collective-permute-start(bf16[512,4]{0,1:T(4,128)(2,1)S(1)} %get-tuple-element.298), channel_id=1, source_target_pairs={{0,4},{4,8},{8,12},{12,16},{16,20},{20,24},{24,28},{1,5},{5,9},{9,... | collective-permute-start | bytes 12296 | tf_op jit(solution)/shard_map/while/body/eval_jaxpr/ppermute | solution.py:19
  197.3 12.8 %collective-permute-start = (bf16[512,256]{0,1:T(8,128)(2,1)}, bf16[512,256]{0,1:T(8,128)(2,1)S(1)}, u32[]{:S(2)}, u32[]{:S(2)}) collective-permute-start(bf16[512,256]{0,1:T(8,128)(2,1)} %get-tuple-element.296), channel_id=1, source_target_pairs={{0,4},{4,8},{8,12},{12,16},{16,20},{20,24},{24,28},{1,5},{5,9},{9,... | collective-permute-start | bytes 786440 | tf_op jit(solution)/shard_map/while/body/eval_jaxpr/ppermute | solution.py:19
  198.6 11.5 %collective-permute-start.2 = (bf16[512,256]{0,1:T(8,128)(2,1)S(1)}, bf16[512,256]{0,1:T(8,128)(2,1)S(1)}, u32[]{:S(2)}, u32[]{:S(2)}) collective-permute-start(bf16[512,256]{0,1:T(8,128)(2,1)S(1)} %get-tuple-element.297), channel_id=1, source_target_pairs={{0,4},{4,8},{8,12},{12,16},{16,20},{20,24},{24,28},{1,5},{5,9},{9,... | collective-permute-start | bytes 786440 | tf_op jit(solution)/shard_map/while/body/eval_jaxpr/ppermute | solution.py:19
  199.9 10.2 %collective-permute-start.1 = (bf16[512,4]{0,1:T(4,128)(2,1)S(1)}, bf16[512,4]{0,1:T(4,128)(2,1)S(1)}, u32[]{:S(2)}, u32[]{:S(2)}) collective-permute-start(bf16[512,4]{0,1:T(4,128)(2,1)S(1)} %get-tuple-element.298), channel_id=1, source_target_pairs={{0,4},{4,8},{8,12},{12,16},{16,20},{20,24},{24,28},{1,5},{5,9},{9,... | collective-permute-start | bytes 12296 | tf_op jit(solution)/shard_map/while/body/eval_jaxpr/ppermute | solution.py:19
  226.2 12.0 %collective-permute-start = (bf16[512,256]{0,1:T(8,128)(2,1)}, bf16[512,256]{0,1:T(8,128)(2,1)S(1)}, u32[]{:S(2)}, u32[]{:S(2)}) collective-permute-start(bf16[512,256]{0,1:T(8,128)(2,1)} %get-tuple-element.296), channel_id=1, source_target_pairs={{0,4},{4,8},{8,12},{12,16},{16,20},{20,24},{24,28},{1,5},{5,9},{9,... | collective-permute-start | bytes 786440 | tf_op jit(solution)/shard_map/while/body/eval_jaxpr/ppermute | solution.py:19
  227.5 10.7 %collective-permute-start.2 = (bf16[512,256]{0,1:T(8,128)(2,1)S(1)}, bf16[512,256]{0,1:T(8,128)(2,1)S(1)}, u32[]{:S(2)}, u32[]{:S(2)}) collective-permute-start(bf16[512,256]{0,1:T(8,128)(2,1)S(1)} %get-tuple-element.297), channel_id=1, source_target_pairs={{0,4},{4,8},{8,12},{12,16},{16,20},{20,24},{24,28},{1,5},{5,9},{9,... | collective-permute-start | bytes 786440 | tf_op jit(solution)/shard_map/while/body/eval_jaxpr/ppermute | solution.py:19
  228.8 9.3 %collective-permute-start.1 = (bf16[512,4]{0,1:T(4,128)(2,1)S(1)}, bf16[512,4]{0,1:T(4,128)(2,1)S(1)}, u32[]{:S(2)}, u32[]{:S(2)}) collective-permute-start(bf16[512,4]{0,1:T(4,128)(2,1)S(1)} %get-tuple-element.298), channel_id=1, source_target_pairs={{0,4},{4,8},{8,12},{12,16},{16,20},{20,24},{24,28},{1,5},{5,9},{9,... | collective-permute-start | bytes 12296 | tf_op jit(solution)/shard_map/while/body/eval_jaxpr/ppermute | solution.py:19
  254.3 11.1 %collective-permute-start = (bf16[512,256]{0,1:T(8,128)(2,1)}, bf16[512,256]{0,1:T(8,128)(2,1)S(1)}, u32[]{:S(2)}, u32[]{:S(2)}) collective-permute-start(bf16[512,256]{0,1:T(8,128)(2,1)} %get-tuple-element.296), channel_id=1, source_target_pairs={{0,4},{4,8},{8,12},{12,16},{16,20},{20,24},{24,28},{1,5},{5,9},{9,... | collective-permute-start | bytes 786440 | tf_op jit(solution)/shard_map/while/body/eval_jaxpr/ppermute | solution.py:19
  255.6 9.8 %collective-permute-start.2 = (bf16[512,256]{0,1:T(8,128)(2,1)S(1)}, bf16[512,256]{0,1:T(8,128)(2,1)S(1)}, u32[]{:S(2)}, u32[]{:S(2)}) collective-permute-start(bf16[512,256]{0,1:T(8,128)(2,1)S(1)} %get-tuple-element.297), channel_id=1, source_target_pairs={{0,4},{4,8},{8,12},{12,16},{16,20},{20,24},{24,28},{1,5},{5,9},{9,... | collective-permute-start | bytes 786440 | tf_op jit(solution)/shard_map/while/body/eval_jaxpr/ppermute | solution.py:19
  256.9 8.5 %collective-permute-start.1 = (bf16[512,4]{0,1:T(4,128)(2,1)S(1)}, bf16[512,4]{0,1:T(4,128)(2,1)S(1)}, u32[]{:S(2)}, u32[]{:S(2)}) collective-permute-start(bf16[512,4]{0,1:T(4,128)(2,1)S(1)} %get-tuple-element.298), channel_id=1, source_target_pairs={{0,4},{4,8},{8,12},{12,16},{16,20},{20,24},{24,28},{1,5},{5,9},{9,... | collective-permute-start | bytes 12296 | tf_op jit(solution)/shard_map/while/body/eval_jaxpr/ppermute | solution.py:19
  281.7 6.2 %collective-permute-start.3 = (bf16[2,2,256]{2,1,0:T(2,128)(2,1)S(1)}, bf16[2,2,256]{2,1,0:T(2,128)(2,1)S(1)}, u32[]{:S(2)}, u32[]{:S(2)}) collective-permute-start(bf16[2,2,256]{2,1,0:T(2,128)(2,1)S(1)} %pad_maximum_fusion.1), channel_id=1, source_target_pairs={{0,4},{4,8},{8,12},{12,16},{16,20},{20,24},{24,28},{1,5},{5,9},{9,... | collective-permute-start | bytes 6152 | tf_op jit(solution)/shard_map/ppermute | solution.py:19
  283.3 4.5 %copy-start.8 = (bf16[512,1536]{1,0:T(8,128)(2,1)S(1)}, bf16[512,1536]{1,0:T(8,128)(2,1)}, u32[]{:S(2)}) copy-start(bf16[512,1536]{1,0:T(8,128)(2,1)} %copy-done.7) | copy-start | bytes 4718596
Sparse Core Ops, SparseCore 0:
  8.9 35.7 all-gather.1
  299.7 51.0 reduce-scatter.1
where the time goes:
time: 361 us; the launch traced here: 358 us
  waiting for transfers between devices  142 us (39%)
  other arithmetic  78.7 us (22%)
  matrix products  68.1 us (19%)
  starting transfers between devices  28.7 us (8%)
  local copies, waits for them, and re-layouts  25.6 us (7%)
  between operations  13.6 us (4%)
    ppermute x22, waiting for transfers between devices, from_behind(): return lax.ppermute(shard, axis, pairs)  66.7 us
    reduce_scatter x1, waiting for transfers between devices, per_device(): lax.psum_scatter(out_terms.astype(jnp.bfloat16), 'tp', scatter_dimension=...  51.2 us
    reduce_sum x8, other arithmetic, stick_terms(): return (result, survival + jnp.sum(totals, axis=-1))  47 us
    ppermute x22, starting transfers between devices, from_behind(): return lax.ppermute(shard, axis, pairs)  28.7 us
    dot_general x8, matrix products, stick_terms(): jnp.einsum('hqbj,js->hqbs', pieces, after_mat, precision=lax.Precision.HI...  24.3 us
    all_gather x1, waiting for transfers between devices, per_device(): gathered = lax.all_gather(tokens, 'tp', axis=1, tiled=True)  23.7 us
    reduce_sum x8, other arithmetic, stick_terms(): totals = jnp.sum(pieces, axis=-1)  22.7 us
    dot_general x8, matrix products, stick_terms(): jnp.einsum('qhe,khe->hqk', queries, key_heads, preferred_element_type=jnp...  17.1 us
  transfers between devices with their start and end apart: 24, of which 9 were waited for; matrix products, arithmetic and copies ran while one was open for 5% of the time, Pallas kernels for 0%

commit v1 on v0

v1 whole, which is shorter than its diff:
```python
import functools
import math

import jax
import jax.numpy as jnp
from jax import lax
from jax.experimental import pallas as pl
from jax.experimental.pallas import tpu as pltpu
from jax.sharding import PartitionSpec as P

HEAD = 64
STICK_HEADS = 16
CONV_WIDTH = 3
MESH = pl.DeviceIdType.MESH
LOG2E = math.log2(math.e)
SPAN = 256


eps = 1e-06


def from_behind(shard, axis, by):
    count = lax.axis_size(axis)
    pairs = [(i, i + by) for i in range(count) if 0 <= i + by < count]
    return lax.ppermute(shard, axis, pairs)


def plane_width(count):
    width = 1
    for w in range(1, count + 1):
        if count % w == 0 and w * w <= count:
            width = w
    return width


def attend_kernel(
    n,
    wide,
    q_ref,
    k_ref,
    v_ref,
    gain_ref,
    out_ref,
    kbuf,
    vbuf,
    qaug,
    tri,
    carry,
    acc,
    send_sem,
    recv_sem,
):
    rows, cols = q_ref.shape
    heads = cols // HEAD
    deep = n // wide
    me = lax.axis_index("sp")
    z, y = me // wide, me % wide

    barrier = pltpu.get_barrier_semaphore()

    def greet(cond, dev):
        @pl.when(cond)
        def _():
            pl.semaphore_signal(barrier, inc=1, device_id={"sp": dev}, device_id_type=MESH)

    greet(z > 0, me - wide)
    greet(z < deep - 1, me + wide)
    for other in range(wide):
        greet(y != other, z * wide + other)

    def copies(ksrc, vsrc, slot, m, way, dev):
        return [
            pltpu.make_async_remote_copy(
                src_ref=src,
                dst_ref=buf.at[slot],
                send_sem=send_sem.at[m, way, part],
                recv_sem=recv_sem.at[slot, part],
                device_id={"sp": dev},
                device_id_type=MESH,
            )
            for part, (src, buf) in enumerate(((ksrc, kbuf), (vsrc, vbuf)))
        ]

    def forward(ksrc, vsrc, m, act):
        slot = me - wide * m

        @pl.when(z < deep - 1)
        def _():
            for c in copies(ksrc, vsrc, slot, m, 0, me + wide):
                act(c)

        for other in range(wide):
            dev = z * wide + other

            @pl.when((y != other) & (slot < dev))
            def _():
                for c in copies(ksrc, vsrc, slot, m, 1 + other, dev):
                    act(c)

    def arrive(slot):
        for c in copies(kbuf.at[slot], vbuf.at[slot], slot, 0, 0, me):
            c.wait_recv()

    for h in range(heads):
        scaled = q_ref[:, h * HEAD : (h + 1) * HEAD].astype(jnp.float32) * (
            HEAD ** (-0.5) * LOG2E
        )
        high = scaled.astype(jnp.bfloat16)
        low = (scaled - high.astype(jnp.float32)).astype(jnp.bfloat16)
        extra = k_ref.shape[0] - cols
        lane = lax.broadcasted_iota(jnp.int32, (rows, extra), 1)
        ones = ((lane >= 2 * h) & (lane < 2 * h + 2)).astype(jnp.float32).astype(jnp.bfloat16)
        qaug[h] = jnp.concatenate([high, low, ones], axis=1)
    carry[...] = jnp.zeros_like(carry)
    acc[...] = jnp.zeros_like(acc)
    above = lax.broadcasted_iota(jnp.int32, (SPAN, SPAN), 0)
    below = lax.broadcasted_iota(jnp.int32, (SPAN, SPAN), 1)
    tri[...] = (above > below).astype(jnp.float32).astype(jnp.bfloat16)

    ends = 1 if deep > 1 else 0
    inner = (z > 0) & (z < deep - 1)

    @pl.when(inner)
    def _():
        pl.semaphore_wait(barrier, wide + 1)

    @pl.when(jnp.logical_not(inner))
    def _():
        pl.semaphore_wait(barrier, wide - 1 + ends)

    forward(k_ref, v_ref, 0, lambda c: c.start())

    def tile(q0, keys, vals, k0, diag):
        for h in range(heads):
            key = keys[h * HEAD : (h + 1) * HEAD, k0 : k0 + SPAN]
            key = jnp.concatenate([key, key, keys[cols:, k0 : k0 + SPAN]], axis=0)
            at = pl.ds(q0, SPAN)
            score = jnp.dot(qaug[h, at, :], key, preferred_element_type=jnp.float32)
            grow = jnp.exp2(jnp.minimum(score, 64.0))
            soft = jnp.maximum(score, jnp.log(1.0 + grow) * LOG2E)
            if diag:
                soft = jnp.where(below < above, soft, 0.0)
            high = soft.astype(jnp.bfloat16)
            low = (soft - high.astype(jnp.float32)).astype(jnp.bfloat16)
            cum = jnp.dot(high, tri[...], preferred_element_type=jnp.float32)
            cum = cum + jnp.dot(low, tri[...], preferred_element_type=jnp.float32)
            held = carry[h, at, :]
            after = jnp.concatenate([held] * (SPAN // 128), axis=1)
            weight = jnp.exp2((score - soft) - cum - after)
            if diag:
                weight = jnp.where(below < above, weight, 0.0)
            acc[h, at, :] += jnp.dot(
                weight.astype(jnp.bfloat16),
                vals[k0 : k0 + SPAN, h * HEAD : (h + 1) * HEAD],
                preferred_element_type=jnp.float32,
            )
            total = cum[:, :1] + soft[:, :1]
            carry[h, at, :] = held + total

    parts = rows // SPAN
    for qi in range(parts):
        for ki in reversed(range(qi + 1)):
            tile(qi * SPAN, k_ref, v_ref, ki * SPAN, qi == ki)

    def earlier(off, none):
        slot = me - off
        m = (off - 1) // wide + 1

        @pl.when(((off - 1) % wide == 0) & (me - wide * m >= 0))
        def _():
            ahead = me - wide * m
            arrive(ahead)
            forward(kbuf.at[ahead], vbuf.at[ahead], m, lambda c: c.start())

        @pl.when(off % wide != 0)
        def _():
            arrive(slot)

        @pl.loop(0, parts)
        def _(qi):
            q0 = pl.multiple_of(qi * SPAN, SPAN)
            for ki in reversed(range(parts)):
                tile(q0, kbuf.at[slot], vbuf.at[slot], ki * SPAN, False)

        return none

    lax.fori_loop(1, me + 1, earlier, 0)

    for h in range(heads):
        at = slice(h * HEAD, (h + 1) * HEAD)
        got = acc[h]
        got = got * lax.rsqrt(jnp.mean(got * got, axis=-1, keepdims=True) + eps)
        out_ref[:, at] = (got * gain_ref[:, at]).astype(out_ref.dtype)

    forward(k_ref, v_ref, 0, lambda c: c.wait_send())

    def sent(m, none):
        slot = me - wide * m
        forward(kbuf.at[slot], vbuf.at[slot], m, lambda c: c.wait_send())
        return none

    lax.fori_loop(1, z + 1, sent, 0)


def attend(queries, keys, values, gain, n):
    rows, cols = queries.shape
    heads = cols // HEAD
    wide = plane_width(n)
    depth = 2 * HEAD + keys.shape[0] - cols
    vmem = pl.BlockSpec(memory_space=pltpu.VMEM)
    return pl.pallas_call(
        functools.partial(attend_kernel, n, wide),
        name="attend",
        out_shape=jax.ShapeDtypeStruct((rows, cols), jnp.bfloat16),
        in_specs=[vmem] * 4,
        out_specs=vmem,
        scratch_shapes=[
            pltpu.VMEM((n,) + keys.shape, jnp.bfloat16),
            pltpu.VMEM((n,) + values.shape, jnp.bfloat16),
            pltpu.VMEM((heads, rows, depth), jnp.bfloat16),
            pltpu.VMEM((SPAN, SPAN), jnp.bfloat16),
            pltpu.VMEM((heads, rows, 128), jnp.float32),
            pltpu.VMEM((heads, rows, HEAD), jnp.float32),
            pltpu.SemaphoreType.DMA((n // wide, 1 + wide, 2)),
            pltpu.SemaphoreType.DMA((n, 2)),
        ],
        compiler_params=pltpu.CompilerParams(
            collective_id=0, has_side_effects=True, vmem_limit_bytes=40 * 1024 * 1024
        ),
    )(queries, keys, values, gain)


def group_norm(value_matrix, gain):
    tok_rows = value_matrix.shape[0]
    grouped = value_matrix.reshape(tok_rows, -1, HEAD)
    grouped = grouped * lax.rsqrt(jnp.mean(grouped * grouped, axis=-1, keepdims=True) + eps)
    return grouped.reshape(tok_rows, -1) * gain


def per_device(
    tokens,
    norm_gain,
    w_query,
    w_key,
    w_value,
    w_gate_out,
    w_gate_in,
    w_conv_in,
    conv_taps,
    key_bias,
    mix_gain,
    out_attn,
    out_conv,
):
    tok_rows = tokens.shape[0]
    head_cols = w_query.shape[1]
    head_count = head_cols // HEAD
    chan_count = w_conv_in.shape[1]
    tp_index = lax.axis_index("tp")
    sp_count = lax.axis_size("sp")
    gathered = lax.all_gather(tokens, "tp", axis=1, tiled=True)
    tok_float = gathered.astype(jnp.float32)
    row_scale = lax.rsqrt(jnp.mean(tok_float * tok_float, axis=1, keepdims=True) + eps)
    normed = (tok_float * row_scale * norm_gain).astype(jnp.bfloat16)

    def project(weight):
        return jnp.dot(normed, weight, preferred_element_type=jnp.float32).astype(jnp.bfloat16)

    queries = project(w_query)
    key_cols = lax.dot_general(
        w_key, normed, (((0,), (1,)), ((), ())), preferred_element_type=jnp.float32
    ).astype(jnp.bfloat16)
    value_rows = project(w_value)
    gate_out = project(w_gate_out)
    gate_in = project(w_gate_in)
    conv_in = project(w_conv_in)
    bias = jnp.transpose(key_bias.astype(jnp.float32)) * LOG2E
    bias_high = lax.reduce_precision(bias, 8, 7)
    bias_low = bias - bias_high
    extra = jnp.stack([bias_high, bias_low], axis=1).reshape(2 * head_count, tok_rows)
    extra = jnp.pad(extra, ((0, -2 * head_count % 16), (0, 0))).astype(jnp.bfloat16)
    keys = jnp.concatenate([key_cols, extra], axis=0)
    attn_gain = lax.dynamic_slice_in_dim(mix_gain, tp_index * head_cols, head_cols)
    attn_normed = attend(queries, keys, value_rows, attn_gain[None, :], sp_count)
    edge_rows = CONV_WIDTH - 1
    tail_rows = jnp.stack([gate_in[tok_rows - edge_rows :], conv_in[tok_rows - edge_rows :]])
    before = from_behind(tail_rows, "sp", 1)
    mixed_in = gate_in.astype(jnp.float32) * conv_in.astype(jnp.float32)
    earlier_mixed = before[0].astype(jnp.float32) * before[1].astype(jnp.float32)
    padded = jnp.concatenate([earlier_mixed, mixed_in], axis=0)
    own_taps = lax.dynamic_slice_in_dim(conv_taps, tp_index * chan_count, chan_count, 1)
    convolved = jnp.zeros((tok_rows, chan_count), jnp.float32)
    for tap_index in range(CONV_WIDTH):
        convolved = convolved + own_taps[tap_index] * padded[tap_index : tap_index + tok_rows]
    conv_out = gate_out.astype(jnp.float32) * convolved
    conv_gain = lax.dynamic_slice_in_dim(
        mix_gain, STICK_HEADS * HEAD + tp_index * chan_count, chan_count
    )
    conv_normed = group_norm(conv_out, conv_gain).astype(jnp.bfloat16)
    out_terms = jnp.dot(attn_normed, out_attn, preferred_element_type=jnp.float32)
    out_terms = out_terms + jnp.dot(conv_normed, out_conv, preferred_element_type=jnp.float32)
    return lax.psum_scatter(out_terms.astype(jnp.bfloat16), "tp", scatter_dimension=1, tiled=True)


def solution(mesh):
    in_specs = (
        P("sp", "tp"),
        P(),
        P(None, "tp"),
        P(None, "tp"),
        P(None, "tp"),
        P(None, "tp"),
        P(None, "tp"),
        P(None, "tp"),
        P(),
        P("sp", "tp"),
        P(),
        P("tp", None),
        P("tp", None),
    )
    out_specs = P("sp", "tp")
    return jax.shard_map(
        per_device, mesh=mesh, in_specs=in_specs, out_specs=out_specs, check_vma=False
    )
```

time: 361 us -> 197 us (0.55)
  Pallas kernels: 0 us -> 76.7 us
  other arithmetic: 78.7 us -> 5.75 us
  waiting for transfers between devices: 142 us -> 81.7 us
  matrix products: 68.1 us -> 12.4 us
  starting transfers between devices: 28.7 us -> 1.33 us
  local copies, waits for them, and re-layouts: 25.6 us -> 3.46 us
    pallas_call x0 -> x1, Pallas kernels: none -> 76.7 us  [attend(): pl.pallas_call(functools.partial(attend_kernel, n, wide), name='attend',...]
    reduce_sum x18 -> x0, other arithmetic: 70.9 us -> none  [the longest x8 47 us: stick_terms(): return (result, survival + jnp.sum(totals, axis=-1))]
    ppermute x22 -> x1, waiting for transfers between devices: 66.7 us -> 0.01 us  [from_behind(): return lax.ppermute(shard, axis, pairs)]
    dot_general x33 -> x6, matrix products: 56.4 us -> 7.92 us  [the longest x5 6.6 us: project(): jnp.dot(normed, weight, preferred_element_type=jnp.float32)]
    ppermute x22 -> x1, starting transfers between devices: 28.7 us -> 1.29 us  [from_behind(): return lax.ppermute(shard, axis, pairs)]
    all_gather x1, waiting for transfers between devices: 23.7 us -> 35 us  [per_device(): gathered = lax.all_gather(tokens, 'tp', axis=1, tiled=True)]
    unnamed x26 -> x20, local copies, waits for them, and re-layouts: 12.2 us -> 1.67 us
    reduce_scatter x1, waiting for transfers between devices: 51.2 us -> 46 us  [per_device(): lax.psum_scatter(out_terms.astype(jnp.bfloat16), 'tp', scatter_dimension=...]
  transfers between devices with their start and end apart: 24 -> 3, of which waited for: 9 -> 2; matrix products, arithmetic and copies ran while one was open for 5% -> 2% of each run, Pallas kernels for 0% -> 39%
where the time goes in v1:
time: 197 us; the launch traced here: 195 us
  waiting for transfers between devices  81.7 us (41%)
  Pallas kernels  76.7 us (39%)
  between operations  13.6 us (7%)
  matrix products  12.4 us (6%)
  other arithmetic  5.75 us (3%)
  local copies, waits for them, and re-layouts  3.46 us (2%)
    pallas_call x1, Pallas kernels, attend(): pl.pallas_call(functools.partial(attend_kernel, n, wide), name='attend',...  76.7 us
    reduce_scatter x1, waiting for transfers between devices, per_device(): lax.psum_scatter(out_terms.astype(jnp.bfloat16), 'tp', scatter_dimension=...  46 us
    all_gather x1, waiting for transfers between devices, per_device(): gathered = lax.all_gather(tokens, 'tp', axis=1, tiled=True)  35 us
    dot_general x5, matrix products, project(): jnp.dot(normed, weight, preferred_element_type=jnp.float32)  6.6 us
  transfers between devices with their start and end apart: 3, of which 2 were waited for; matrix products, arithmetic and copies ran while one was open for 2% of the time, Pallas kernels for 39%

profile of v1, /device:TPU:29, one launch (start us, length us, event | category | flops | bytes accessed | tf_op | source)
XLA Modules:
  0.0 195.1 jit_solution(898923009353706104)
XLA Ops:
  6.5 0.0 copy-start
  6.5 0.0 copy-start.3
  6.5 0.0 all-gather.2.cloned.1.call-start
  6.5 0.7 all-gather.2.cloned.1.call-update
  7.3 0.0 reduce-scatter.2.cloned.1.call-start
  7.3 0.7 fusion.17
  8.1 0.8 fusion.18
  8.8 0.9 constant_dynamic-slice_fusion
  9.7 35.0 %all-gather.2.cloned.1.call-done = bf16[512,4096]{1,0:T(8,128)(2,1)} async-done(((bf16[512,1024]{1,0:T(8,128)(2,1)}), bf16[512,4096]{1,0:T(8,128)(2,1)}) %all-gather.2.cloned.1.call-update) | async-done | bytes 4194320 | tf_op jit(solution)/shard_map/all_gather | solution.py:261
  44.7 0.0 copy-start.1
  44.7 3.2 %fusion = f32[512]{0:T(512)S(1)} fusion(bf16[512,4096]{1,0:T(8,128)(2,1)} %all-gather.2.cloned.1.call-done), kind=kLoop, calls=%fused_computation.2 | loop fusion | flops 6290944 | bytes 4196352 | tf_op jit(solution)/shard_map/reduce_sum | solution.py:263
  48.0 0.0 copy-done.3
  48.0 0.2 copy-done.1
  48.2 0.0 copy-start.4
  48.2 1.6 fusion.2
  49.8 0.0 copy-done.4
  49.8 0.0 copy-start.5
  49.8 1.3 convolution_convert_fusion.1
  51.1 0.3 copy-done.5
  51.4 0.0 copy-start.6
  51.4 1.3 convolution_convert_fusion.3.v_ref
  52.7 0.3 copy-done.6
  53.0 0.0 copy-start.7
  53.0 1.3 fusion.5
  54.3 0.3 copy-done.7
  54.6 0.0 copy-start.8
  54.6 1.3 convolution_convert_fusion.5.q_ref
  55.9 0.3 copy-done.8
  56.2 1.3 convert_multiply_fusion.2
  57.5 0.1 slice_bitcast_fusion
  57.7 1.3 collective-permute-start
  59.0 76.7 %attend.1 = bf16[512,256]{1,0:T(8,128)(2,1)S(1)} custom-call(bf16[512,256]{1,0:T(8,128)(2,1)S(1)} %convolution_convert_fusion.5.q_ref, bf16[272,512]{1,0:T(8,128)(2,1)S(1)} %fusion.14.k_ref, bf16[512,256]{1,0:T(8,128)(2,1)S(1)} %convolution_convert_fusion.3.v_ref, f32[1,256]{1,0:T(1,128)S(1)} %bitcast.47), custom_call_target="tpu_custom_call" | custom-call | tf_op jit(solution)/shard_map/attend/pallas_call | solution.py:211
  135.7 0.0 copy-done
  135.7 0.0 copy-start.9
  135.8 1.3 fusion.19
  137.0 0.0 collective-permute-done
  137.1 0.3 copy-done.9
  137.3 0.0 copy-start.2
  137.3 1.4 bitcast_reduce_fusion
  138.8 0.1 fusion.13
  138.9 0.0 copy-done.2
  138.9 3.2 %add_convert_fusion = bf16[512,4096]{1,0:T(8,128)(2,1)} fusion(f32[512,4096]{1,0:T(8,128)S(1)} %fusion.19, bf16[512,256]{0,1:T(8,128)(2,1)S(1)} %fusion.13, bf16[256,4096]{1,0:T(8,128)(2,1)S(1)} %copy-done.2), kind=kOutput, calls=%fused_computation.5 | convolution fusion | flops 1077936128 | bytes 14942208 | tf_op jit(solution)/shard_map/dot_general | solution.py:301
  142.2 0.0 reduce-scatter.2.cloned.1.call-update
  142.2 46.0 %reduce-scatter.2.cloned.1.call-done = bf16[512,1024]{1,0:T(8,128)(2,1)} async-done(((bf16[512,4096]{1,0:T(8,128)(2,1)}), bf16[512,1024]{1,0:T(8,128)(2,1)}) %reduce-scatter.2.cloned.1.call-update) | async-done | bytes 1048592 | tf_op jit(solution)/shard_map/reduce_scatter | solution.py:302
  (8 shorter events, 0.1 us)
Async XLA Ops:
  6.5 129.2 %copy-start = (bf16[256,4096]{1,0:T(8,128)(2,1)S(1)}, bf16[256,4096]{1,0:T(8,128)(2,1)}, u32[]{:S(2)}) copy-start(bf16[256,4096]{1,0:T(8,128)(2,1)} %param.24) | copy-start | bytes 6291460
  6.5 41.4 %copy-start.3 = (f32[4096]{0:T(1024)S(1)}, f32[4096]{0:T(1024)}, u32[]{:S(2)}) copy-start(f32[4096]{0:T(1024)} %param.14) | copy-start | bytes 49156
  6.5 38.2 %all-gather.2.cloned.1.call-start = ((), (), s32[]{:S(2)}) async-start(), calls=%async_computation.1 | async-start | bytes 5242880 | tf_op jit(solution)/shard_map/all_gather | solution.py:261
  7.3 181.0 %reduce-scatter.2.cloned.1.call-start = ((), (), s32[]{:S(2)}) async-start(), calls=%async_computation.2 | async-start | bytes 5242880 | tf_op jit(solution)/shard_map/reduce_scatter | solution.py:302
  44.7 3.4 %copy-start.1 = (bf16[512,4096]{1,0:T(8,128)(2,1)S(1)}, bf16[512,4096]{1,0:T(8,128)(2,1)}, u32[]{:S(2)}) copy-start(bf16[512,4096]{1,0:T(8,128)(2,1)} %all-gather.2.cloned.1.call-done) | copy-start | bytes 12582916
  48.2 1.6 copy-start.4
  49.8 1.6 copy-start.5
  51.4 1.6 copy-start.6
  53.0 1.6 copy-start.7
  54.6 1.6 copy-start.8
  57.7 79.4 %collective-permute-start = (bf16[2,2,256]{1,2,0:T(8,128)(2,1)S(1)}, bf16[2,2,256]{1,2,0:T(8,128)(2,1)S(1)}, u32[]{:S(2)}, u32[]{:S(2)}) collective-permute-start(bf16[2,2,256]{1,2,0:T(8,128)(2,1)S(1)} %pad_maximum_fusion.1), channel_id=1, source_target_pairs={{0,4},{4,8},{8,12},{12,16},{16,20},{20,24},{24,28},{1,5},{5,9},{9,... | collective-permute-start | bytes 6152 | tf_op jit(solution)/shard_map/ppermute | solution.py:25
  135.7 1.6 copy-start.9
  137.3 1.6 copy-start.2
Sparse Core Ops, SparseCore 0:
  8.9 35.7 all-gather.1
  142.3 45.8 reduce-scatter.1

commit v2 on v1

--- a/solution.py
+++ b/solution.py
@@ -36,10 +36,14 @@
 def attend_kernel(
     n,
     wide,
+    tp,
     q_ref,
     k_ref,
     v_ref,
     gain_ref,
+    conv_ref,
+    wattn_ref,
+    wconv_ref,
     out_ref,
     kbuf,
     vbuf,
@@ -47,14 +51,27 @@
     tri,
     carry,
     acc,
+    wbuf,
+    mixbuf,
+    own_attn,
+    total_ref,
     send_sem,
     recv_sem,
+    wsend_sem,
+    wrecv_sem,
+    msend_sem,
+    mrecv_sem,
 ):
     rows, cols = q_ref.shape
     heads = cols // HEAD
     deep = n // wide
     me = lax.axis_index("sp")
     z, y = me // wide, me % wide
+    tme = lax.axis_index("tp")
+    chips = tp // 2
+    chip, core = tme // 2, tme % 2
+    mate = chip * 2 + (1 - core)
+    width = out_ref.shape[1]
 
     barrier = pltpu.get_barrier_semaphore()
 
@@ -67,6 +84,77 @@
     greet(z < deep - 1, me + wide)
     for other in range(wide):
         greet(y != other, z * wide + other)
+
+    for t in range(tp):
+
+        @pl.when(tme != t)
+        def _():
+            pl.semaphore_signal(barrier, inc=1, device_id={"tp": t}, device_id_type=MESH)
+
+    def weight_copies(t, part):
+        src = (wattn_ref, wconv_ref)[part]
+        return pltpu.make_async_remote_copy(
+            src_ref=src.at[:, pl.ds(t * width, width)],
+            dst_ref=wbuf.at[part, tme],
+            send_sem=wsend_sem.at[part, t],
+            recv_sem=wrecv_sem.at[part, tme],
+            device_id={"tp": t},
+            device_id_type=MESH,
+        )
+
+    def weight_copies_in(t, part):
+        src = (wattn_ref, wconv_ref)[part]
+        pltpu.make_async_remote_copy(
+            src_ref=src.at[:, pl.ds(0, width)],
+            dst_ref=wbuf.at[part, t],
+            send_sem=wsend_sem.at[part, t],
+            recv_sem=wrecv_sem.at[part, t],
+            device_id={"tp": t},
+            device_id_type=MESH,
+        ).wait_recv()
+
+    def own_weights(part):
+        src = (wattn_ref, wconv_ref)[part]
+        return pltpu.make_async_copy(
+            src.at[:, pl.ds(pl.multiple_of(tme * width, width), width)],
+            wbuf.at[part, tme],
+            wsend_sem.at[part, tp],
+        )
+
+    def mix_copy(src, part, slot, way, dev):
+        return pltpu.make_async_remote_copy(
+            src_ref=src,
+            dst_ref=mixbuf.at[part, slot],
+            send_sem=msend_sem.at[part, way],
+            recv_sem=mrecv_sem.at[part, slot],
+            device_id={"tp": dev},
+            device_id_type=MESH,
+        )
+
+    def spread(src, part, act):
+        for other in range(chips):
+
+            @pl.when(chip != other)
+            def _():
+                act(mix_copy(src, part, tme, other, other * 2 + core))
+
+        act(mix_copy(src, part, tme, chips, mate))
+
+    def relay(part, act):
+        for other in range(chips):
+
+            @pl.when(chip != other)
+            def _():
+                slot = other * 2 + core
+                act(mix_copy(mixbuf.at[part, slot], part, slot, chips + 1 + other, mate))
+
+    def arrive_relayed(part):
+        for other in range(chips):
+
+            @pl.when(chip != other)
+            def _():
+                slot = other * 2 + core
+                mix_copy(mixbuf.at[part, slot], part, slot, 0, mate).wait_recv()
 
     def copies(ksrc, vsrc, slot, m, way, dev):
         return [
@@ -122,13 +210,23 @@
 
     @pl.when(inner)
     def _():
-        pl.semaphore_wait(barrier, wide + 1)
+        pl.semaphore_wait(barrier, wide + tp)
 
     @pl.when(jnp.logical_not(inner))
     def _():
-        pl.semaphore_wait(barrier, wide - 1 + ends)
+        pl.semaphore_wait(barrier, wide + tp - 2 + ends)
 
     forward(k_ref, v_ref, 0, lambda c: c.start())
+    for part in range(2):
+        own_weights(part).start()
+    for part in range(2):
+        for t in range(tp):
+
+            @pl.when(tme != t)
+            def _():
+                weight_copies(t, part).start()
+
+    spread(conv_ref, 1, lambda c: c.start())
 
     def tile(q0, keys, vals, k0, diag):
         for h in range(heads):
@@ -190,7 +288,79 @@
         at = slice(h * HEAD, (h + 1) * HEAD)
         got = acc[h]
         got = got * lax.rsqrt(jnp.mean(got * got, axis=-1, keepdims=True) + eps)
-        out_ref[:, at] = (got * gain_ref[:, at]).astype(out_ref.dtype)
+        own_attn[:, at] = (got * gain_ref[:, at]).astype(own_attn.dtype)
+
+    spread(own_attn, 0, lambda c: c.start())
+    arrive_relayed(1)
+    relay(1, lambda c: c.start())
+    for part in range(2):
+        own_weights(part).wait()
+        for t in range(tp):
+
+            @pl.when(tme != t)
+            def _():
+                weight_copies_in(t, part)
+
+    mix_copy(own_attn, 0, mate, 0, mate).wait_recv()
+    mix_copy(own_attn, 1, mate, 0, mate).wait_recv()
+    for other in range(chips):
+
+        @pl.when(chip != other)
+        def _():
+            slot = other * 2 + 1 - core
+            mix_copy(own_attn, 1, slot, 0, mate).wait_recv()
+
+    step = math.gcd(rows, 128)
+    lanes = math.gcd(width, 256)
+
+    def product(src, at, part, slot, over):
+        return jnp.dot(src[at, :], wbuf[part, slot, :, over], preferred_element_type=jnp.float32)
+
+    @pl.loop(0, rows // step)
+    def _(i):
+        at = pl.ds(pl.multiple_of(i * step, step), step)
+        for j in range(width // lanes):
+            over = slice(j * lanes, (j + 1) * lanes)
+            total = product(own_attn, at, 0, tme, over)
+            total += product(mixbuf.at[0, mate], at, 0, mate, over)
+            total += product(conv_ref, at, 1, tme, over)
+            total += product(mixbuf.at[1, mate], at, 1, mate, over)
+            for k in range(1, chips):
+                for c in range(2):
+                    slot = (chip + k) % chips * 2 + c
+                    total += product(mixbuf.at[1, slot], at, 1, slot, over)
+            total_ref[at, over] = total
+
+    arrive_relayed(0)
+    relay(0, lambda c: c.start())
+    for other in range(chips):
+
+        @pl.when(chip != other)
+        def _():
+            slot = other * 2 + 1 - core
+            mix_copy(own_attn, 0, slot, 0, mate).wait_recv()
+
+    @pl.loop(0, rows // step)
+    def _(i):
+        at = pl.ds(pl.multiple_of(i * step, step), step)
+        for j in range(width // lanes):
+            over = slice(j * lanes, (j + 1) * lanes)
+            total = total_ref[at, over]
+            for k in range(1, chips):
+                for c in range(2):
+                    slot = (chip + k) % chips * 2 + c
+                    total += product(mixbuf.at[0, slot], at, 0, slot, over)
+            out_ref[at, over] = total.astype(out_ref.dtype)
+
+    for part in range(2):
+        for t in range(tp):
+
+            @pl.when(tme != t)
+            def _():
+                weight_copies(t, part).wait_send()
+
+        spread((own_attn, conv_ref)[part], part, lambda c: c.wait_send())
+        relay(part, lambda c: c.wait_send())
 
     forward(k_ref, v_ref, 0, lambda c: c.wait_send())
 
@@ -202,17 +372,19 @@
     lax.fori_loop(1, z + 1, sent, 0)
 
 
-def attend(queries, keys, values, gain, n):
+def attend(queries, keys, values, gain, conv, w_attn, w_conv, n, tp):
     rows, cols = queries.shape
     heads = cols // HEAD
     wide = plane_width(n)
+    width = w_attn.shape[1] // tp
+    any_space = pl.BlockSpec(memory_space=pl.ANY)
     depth = 2 * HEAD + keys.shape[0] - cols
     vmem = pl.BlockSpec(memory_space=pltpu.VMEM)
     return pl.pallas_call(
-        functools.partial(attend_kernel, n, wide),
+        functools.partial(attend_kernel, n, wide, tp),
         name="attend",
-        out_shape=jax.ShapeDtypeStruct((rows, cols), jnp.bfloat16),
-        in_specs=[vmem] * 4,
+        out_shape=jax.ShapeDtypeStruct((rows, width), jnp.bfloat16),
+        in_specs=[vmem] * 5 + [any_space] * 2,
         out_specs=vmem,
         scratch_shapes=[
             pltpu.VMEM((n,) + keys.shape, jnp.bfloat16),
@@ -221,13 +393,21 @@
             pltpu.VMEM((SPAN, SPAN), jnp.bfloat16),
             pltpu.VMEM((heads, rows, 128), jnp.float32),
             pltpu.VMEM((heads, rows, HEAD), jnp.float32),
+            pltpu.VMEM((2, tp, cols, width), jnp.bfloat16),
+            pltpu.VMEM((2, tp, rows, cols), jnp.bfloat16),
+            pltpu.VMEM((rows, cols), jnp.bfloat16),
+            pltpu.VMEM((rows, width), jnp.float32),
             pltpu.SemaphoreType.DMA((n // wide, 1 + wide, 2)),
             pltpu.SemaphoreType.DMA((n, 2)),
+            pltpu.SemaphoreType.DMA((2, tp + 1)),
+            pltpu.SemaphoreType.DMA((2, tp)),
+            pltpu.SemaphoreType.DMA((2, tp + 1)),
+            pltpu.SemaphoreType.DMA((2, tp)),
         ],
         compiler_params=pltpu.CompilerParams(
             collective_id=0, has_side_effects=True, vmem_limit_bytes=40 * 1024 * 1024
         ),
-    )(queries, keys, values, gain)
+    )(queries, keys, values, gain, conv, w_attn, w_conv)
 
 
 def group_norm(value_matrix, gain):
@@ -281,7 +461,6 @@
     extra = jnp.pad(extra, ((0, -2 * head_count % 16), (0, 0))).astype(jnp.bfloat16)
     keys = jnp.concatenate([key_cols, extra], axis=0)
     attn_gain = lax.dynamic_slice_in_dim(mix_gain, tp_index * head_cols, head_cols)
-    attn_normed = attend(queries, keys, value_rows, attn_gain[None, :], sp_count)
     edge_rows = CONV_WIDTH - 1
     tail_rows = jnp.stack([gate_in[tok_rows - edge_rows :], conv_in[tok_rows - edge_rows :]])
     before = from_behind(tail_rows, "sp", 1)
@@ -297,9 +476,17 @@
         mix_gain, STICK_HEADS * HEAD + tp_index * chan_count, chan_count
     )
     conv_normed = group_norm(conv_out, conv_gain).astype(jnp.bfloat16)
-    out_terms = jnp.dot(attn_normed, out_attn, preferred_element_type=jnp.float32)
-    out_terms = out_terms + jnp.dot(conv_normed, out_conv, preferred_element_type=jnp.float32)
-    return lax.psum_scatter(out_terms.astype(jnp.bfloat16), "tp", scatter_dimension=1, tiled=True)
+    return attend(
+        queries,
+        keys,
+        value_rows,
+        attn_gain[None, :],
+        conv_normed,
+        out_attn,
+        out_conv,
+        sp_count,
+        lax.axis_size("tp"),
+    )
 
 
 def solution(mesh):

time: 197 us -> 163 us (0.83)
  waiting for transfers between devices: 81.7 us -> 35.8 us
  Pallas kernels: 76.7 us -> 86.3 us
  local copies, waits for them, and re-layouts: 3.46 us -> 9.94 us
  matrix products: 12.4 us -> 8.7 us
    reduce_scatter x1 -> x0, waiting for transfers between devices: 46 us -> none  [per_device(): lax.psum_scatter(out_terms.astype(jnp.bfloat16), 'tp', scatter_dimension=...]
    pallas_call x1, Pallas kernels: 76.7 us -> 86.3 us  [attend(): pl.pallas_call(functools.partial(attend_kernel, n, wide, tp), name='atten...]
    dot_general x2 -> x0, matrix products: 4.52 us -> none  [the longest x1 3.25 us: per_device(): jnp.dot(conv_normed, out_conv, preferred_element_type=jnp.float32)]
    mul x0 -> x3, local copies, waits for them, and re-layouts: none -> 3.33 us  [the longest x2 2.09 us: group_norm(): grouped * lax.rsqrt(jnp.mean(grouped * grouped, axis=-1, keepdims=True) +...]
    unnamed x20 -> x21, local copies, waits for them, and re-layouts: 1.67 us -> 4.93 us
  transfers between devices with their start and end apart: 3 -> 2, of which waited for: 2 -> 1; matrix products, arithmetic and copies ran while one was open for 2% -> 4% of each run, Pallas kernels for 39% -> 0%
where the time goes in v2:
time: 163 us
  Pallas kernels  86.3 us (53%)
  waiting for transfers between devices  35.8 us (22%)
  between operations  13.6 us (8%)
  local copies, waits for them, and re-layouts  9.94 us (6%)
  matrix products  8.7 us (5%)
  other arithmetic  6.82 us (4%)
    pallas_call x1, Pallas kernels, attend(): pl.pallas_call(functools.partial(attend_kernel, n, wide, tp), name='atten...  86.3 us
    all_gather x1, waiting for transfers between devices, per_device(): gathered = lax.all_gather(tokens, 'tp', axis=1, tiled=True)  35.1 us
    dot_general x5, matrix products, project(): jnp.dot(normed, weight, preferred_element_type=jnp.float32)  7.37 us
    unnamed x21, local copies, waits for them, and re-layouts  4.93 us
  transfers between devices with their start and end apart: 2, of which 1 were waited for; matrix products, arithmetic and copies ran while one was open for 4% of the time, Pallas kernels for 0%

profile of v2, /device:TPU:29, one launch (start us, length us, event | category | flops | bytes accessed | tf_op | source)
XLA Modules:
  0.0 162.6 jit_solution(17586651045292406828)
XLA Ops:
  6.5 0.0 copy-start
  6.5 0.0 copy-start.4
  6.5 0.0 all-gather.2.cloned.1.call-start
  6.5 0.7 all-gather.2.cloned.1.call-update
  7.3 0.7 fusion.15
  8.0 0.8 fusion.16
  8.8 0.9 constant_dynamic-slice_fusion
  9.7 35.1 %all-gather.2.cloned.1.call-done = bf16[512,4096]{1,0:T(8,128)(2,1)} async-done(((bf16[512,1024]{1,0:T(8,128)(2,1)}), bf16[512,4096]{1,0:T(8,128)(2,1)}) %all-gather.2.cloned.1.call-update) | async-done | bytes 4194320 | tf_op jit(solution)/shard_map/all_gather | solution.py:441
  44.8 0.0 copy-start.3
  44.8 3.2 %fusion = f32[512]{0:T(512)S(1)} fusion(bf16[512,4096]{1,0:T(8,128)(2,1)} %all-gather.2.cloned.1.call-done), kind=kLoop, calls=%fused_computation.2 | loop fusion | flops 6290944 | bytes 4196352 | tf_op jit(solution)/shard_map/reduce_sum | solution.py:443
  48.0 0.0 copy-done.4
  48.0 0.2 copy-done.3
  48.2 0.0 copy-start.5
  48.2 1.7 %fusion.2 = bf16[512,4096]{1,0:T(8,128)(2,1)S(1)} fusion(bf16[512,4096]{1,0:T(8,128)(2,1)S(1)} %copy-done.3, f32[4096]{0:T(1024)S(1)} %copy-done.4, f32[512]{0:T(512)S(1)} %add_rsqrt_fusion.1), kind=kLoop, calls=%fused_computation.4 | loop fusion | flops 8388608 | bytes 8407040 | tf_op jit(solution)/shard_map/convert_element_type | solution.py:444
  49.9 0.0 copy-done.5
  49.9 1.2 convolution_convert_fusion.1
  51.1 0.0 copy-done
  51.2 0.0 copy-start.6
  51.2 1.3 convert_multiply_fusion.2
  52.5 0.0 copy-start.7
  52.5 1.4 collective-permute-start
  53.9 0.0 copy-done.6
  53.9 1.3 fusion.5
  55.3 0.0 copy-done.7
  55.3 0.0 copy-start.8
  55.3 1.3 convolution_convert_fusion.3.v_ref
  56.6 0.3 copy-done.8
  56.9 0.0 copy-start.9
  56.9 1.3 convolution_convert_fusion.5.q_ref
  58.2 0.0 collective-permute-done
  58.2 0.3 copy-done.9
  58.5 2.3 %fusion.17 = (f32[512,256]{1,0:T(8,128)}, f32[512,256]{1,0:T(8,128)}) fusion(f32[512,256]{1,0:T(8,128)S(1)} %get-tuple-element.12, f32[256]{0:T(256)S(1)} %bitcast.42, f32[2,256]{1,0:T(2,128)S(1)} %multiply_bitcast_fusion, f32[256]{0:T(256)S(1)} %bitcast.41, f32[256]{0:T(256)S(1)} %bitcast.40, bf16[512,4096]{1,0:T(8,128)(2,1)S(1)} %fusion.2, ...), kind=kOutput, calls=%fused_computation.43 | convolution fusion | flops 1075183616 | bytes 7869440 | tf_op jit(solution)/shard_map/dot_general | solution.py:447
  60.8 1.2 copy.18
  62.0 0.1 bitcast_reduce_fusion
  62.1 0.9 mul.124
  62.9 1.2 copy.19
  64.2 1.1 multiply_convert_fusion.conv_ref
  65.3 0.0 copy-start.1
  65.3 1.6 copy-done.1
  66.9 0.0 copy-start.2
  66.9 1.6 copy-done.2
  68.5 86.3 %attend.1 = bf16[512,1024]{1,0:T(8,128)(2,1)S(1)} custom-call(bf16[512,256]{1,0:T(8,128)(2,1)S(1)} %convolution_convert_fusion.5.q_ref, bf16[272,512]{1,0:T(8,128)(2,1)S(1)} %fusion.12.k_ref, bf16[512,256]{1,0:T(8,128)(2,1)S(1)} %convolution_convert_fusion.3.v_ref, f32[1,256]{1,0:T(1,128)S(1)} %bitcast.38, ...), custom_call_target="tpu_custom_call" | custom-call | tf_op jit(solution)/shard_map/attend/pallas_call | solution.py:383
  154.8 1.0 copy.22
  (9 shorter events, 0.1 us)
Async XLA Ops:
  6.5 44.6 %copy-start = (bf16[4096,256]{1,0:T(8,128)(2,1)S(1)}, bf16[4096,256]{1,0:T(8,128)(2,1)}, u32[]{:S(2)}) copy-start(bf16[4096,256]{1,0:T(8,128)(2,1)} %param.20) | copy-start | bytes 6291460
  6.5 41.5 %copy-start.4 = (f32[4096]{0:T(1024)S(1)}, f32[4096]{0:T(1024)}, u32[]{:S(2)}) copy-start(f32[4096]{0:T(1024)} %param.14) | copy-start | bytes 49156
  6.5 38.2 %all-gather.2.cloned.1.call-start = ((), (), s32[]{:S(2)}) async-start(), calls=%async_computation | async-start | bytes 5242880 | tf_op jit(solution)/shard_map/all_gather | solution.py:441
  44.8 3.4 %copy-start.3 = (bf16[512,4096]{1,0:T(8,128)(2,1)S(1)}, bf16[512,4096]{1,0:T(8,128)(2,1)}, u32[]{:S(2)}) copy-start(bf16[512,4096]{1,0:T(8,128)(2,1)} %all-gather.2.cloned.1.call-done) | copy-start | bytes 12582916
  48.2 1.7 %copy-start.5 = (bf16[4096,256]{1,0:T(8,128)(2,1)S(1)}, bf16[4096,256]{1,0:T(8,128)(2,1)}, u32[]{:S(2)}) copy-start(bf16[4096,256]{1,0:T(8,128)(2,1)} %param.19) | copy-start | bytes 6291460
  51.2 2.8 %copy-start.6 = (bf16[4096,256]{1,0:T(8,128)(2,1)S(1)}, bf16[4096,256]{1,0:T(8,128)(2,1)}, u32[]{:S(2)}) copy-start(bf16[4096,256]{1,0:T(8,128)(2,1)} %param.16) | copy-start | bytes 6291460
  52.5 2.8 %copy-start.7 = (bf16[4096,256]{1,0:T(8,128)(2,1)S(1)}, bf16[4096,256]{1,0:T(8,128)(2,1)}, u32[]{:S(2)}) copy-start(bf16[4096,256]{1,0:T(8,128)(2,1)} %param.17) | copy-start | bytes 6291460
  52.5 5.7 %collective-permute-start = (bf16[2,2,256]{2,1,0:T(2,128)(2,1)S(1)}, bf16[2,2,256]{2,1,0:T(2,128)(2,1)S(1)}, u32[]{:S(2)}, u32[]{:S(2)}) collective-permute-start(bf16[2,2,256]{2,1,0:T(2,128)(2,1)S(1)} %pad_maximum_fusion.2), channel_id=1, source_target_pairs={{0,4},{4,8},{8,12},{12,16},{16,20},{20,24},{24,28},{1,5},{5,9},{9,... | collective-permute-start | bytes 6152 | tf_op jit(solution)/shard_map/ppermute | solution.py:25
  55.3 1.6 copy-start.8
  56.9 1.6 copy-start.9
  65.3 1.6 copy-start.1
  66.9 1.6 copy-start.2
Sparse Core Ops, SparseCore 0:
  8.9 35.8 all-gather.1

commit v3 on v2

--- a/solution.py
+++ b/solution.py
@@ -410,6 +410,143 @@
     )(queries, keys, values, gain, conv, w_attn, w_conv)
 
 
+def project_kernel(
+    tp,
+    tok_ref,
+    gain_ref,
+    extra_ref,
+    *refs,
+):
+    weights, outs = refs[:6], refs[6:12]
+    tokbuf, wbuf, nbuf, load_sem, send_sem, recv_sem = refs[12:]
+    rows, width = tok_ref.shape
+    tme = lax.axis_index("tp")
+    chips = tp // 2
+    chip, core = tme // 2, tme % 2
+    mate = chip * 2 + (1 - core)
+    cut = math.gcd(rows, 128)
+    steps = rows // cut
+
+    barrier = pltpu.get_barrier_semaphore()
+    for t in range(tp):
+
+        @pl.when(tme != t)
+        def _():
+            pl.semaphore_signal(barrier, inc=1, device_id={"tp": t}, device_id_type=MESH)
+
+    loads = [pltpu.make_async_copy(w, wbuf.at[i], load_sem.at[i]) for i, w in enumerate(weights)]
+    pl.semaphore_wait(barrier, tp - 1)
+
+    def copy(src, r, slot, way, dev):
+        at = pl.ds(pl.multiple_of(r * cut, cut), cut)
+        return pltpu.make_async_remote_copy(
+            src_ref=src.at[at, :],
+            dst_ref=tokbuf.at[slot, at, :],
+            send_sem=send_sem.at[r, way],
+            recv_sem=recv_sem.at[r, slot],
+            device_id={"tp": dev},
+            device_id_type=MESH,
+        )
+
+    def spread(r, act):
+        for other in range(chips):
+
+            @pl.when(chip != other)
+            def _():
+                act(copy(tok_ref, r, tme, other, other * 2 + core))
+
+        act(copy(tok_ref, r, tme, chips, mate))
+
+    def relay(r, act):
+        for other in range(chips):
+
+            @pl.when(chip != other)
+            def _():
+                slot = other * 2 + core
+                act(copy(tokbuf.at[slot], r, slot, chips + 1 + other, mate))
+
+    @pl.loop(0, steps)
+    def _(r):
+        spread(r, lambda c: c.start())
+
+    for load in loads:
+        load.start()
+    tokbuf[tme] = tok_ref[...]
+    for load in loads:
+        load.wait()
+    keys = outs[1]
+    cols = outs[0].shape[1]
+    keys[cols:, :] = extra_ref[...]
+
+    for r in range(steps):
+        for other in range(chips):
+
+            @pl.when(chip != other)
+            def _():
+                slot = other * 2 + core
+                copy(tok_ref, r, slot, 0, mate).wait_recv()
+
+        relay(r, lambda c: c.start())
+        copy(tok_ref, r, mate, 0, mate).wait_recv()
+        for other in range(chips):
+
+            @pl.when(chip != other)
+            def _():
+                slot = other * 2 + 1 - core
+                copy(tok_ref, r, slot, 0, mate).wait_recv()
+
+        at = slice(r * cut, (r + 1) * cut)
+        square = jnp.zeros((cut, 128), jnp.float32)
+        for t in range(tp):
+            piece = tokbuf[t, at, :].astype(jnp.float32)
+            piece = piece * piece
+            for i in range(width // 128):
+                square += piece[:, i * 128 : (i + 1) * 128]
+        scale = lax.rsqrt(jnp.sum(square, axis=1, keepdims=True) / (tp * width) + eps)
+        for t in range(tp):
+            over = slice(t * width, (t + 1) * width)
+            piece = tokbuf[t, at, :].astype(jnp.float32) * scale * gain_ref[:, over]
+            nbuf[:, over] = piece.astype(nbuf.dtype)
+        for i, out in enumerate(outs):
+            got = jnp.dot(nbuf[...], wbuf[i], preferred_element_type=jnp.float32)
+            if i == 1:
+                out[:cols, at] = got.T.astype(out.dtype)
+            else:
+                out[at, :] = got.astype(out.dtype)
+
+    @pl.loop(0, steps)
+    def _(r):
+        spread(r, lambda c: c.wait_send())
+        relay(r, lambda c: c.wait_send())
+
+
+def project_all(tokens, gain, extra, weights, tp):
+    rows, width = tokens.shape
+    deep, cols = weights[0].shape
+    steps = rows // math.gcd(rows, 128)
+    vmem = pl.BlockSpec(memory_space=pltpu.VMEM)
+    flat = jax.ShapeDtypeStruct((rows, cols), jnp.bfloat16)
+    turned = jax.ShapeDtypeStruct((cols + extra.shape[0], rows), jnp.bfloat16)
+    return pl.pallas_call(
+        functools.partial(project_kernel, tp),
+        name="front",
+        out_shape=(flat, turned, flat, flat, flat, flat),
+        in_specs=[vmem] * 3 + [pl.BlockSpec(memory_space=pl.ANY)] * 6,
+        out_specs=(vmem,) * 6,
+        scratch_shapes=[
+            pltpu.VMEM((tp, rows, width), jnp.bfloat16),
+            pltpu.VMEM((6, deep, cols), jnp.bfloat16),
+            pltpu.VMEM((rows // steps, deep), jnp.bfloat16),
+            pltpu.SemaphoreType.DMA((6,)),
+            pltpu.SemaphoreType.DMA((steps, tp + 1)),
+            pltpu.SemaphoreType.DMA((steps, tp)),
+        ],
+        compiler_params=pltpu.CompilerParams(
+            collective_id=1, has_side_effects=True, vmem_limit_bytes=40 * 1024 * 1024
+        ),
+    )(tokens, gain, extra, *weights)
+
+
 def group_norm(value_matrix, gain):
     tok_rows = value_matrix.shape[0]
     grouped = value_matrix.reshape(tok_rows, -1, HEAD)
@@ -438,28 +575,18 @@
     chan_count = w_conv_in.shape[1]
     tp_index = lax.axis_index("tp")
     sp_count = lax.axis_size("sp")
-    gathered = lax.all_gather(tokens, "tp", axis=1, tiled=True)
-    tok_float = gathered.astype(jnp.float32)
-    row_scale = lax.rsqrt(jnp.mean(tok_float * tok_float, axis=1, keepdims=True) + eps)
-    normed = (tok_float * row_scale * norm_gain).astype(jnp.bfloat16)
-
-    def project(weight):
-        return jnp.dot(normed, weight, preferred_element_type=jnp.float32).astype(jnp.bfloat16)
-
-    queries = project(w_query)
-    key_cols = lax.dot_general(
-        w_key, normed, (((0,), (1,)), ((), ())), preferred_element_type=jnp.float32
-    ).astype(jnp.bfloat16)
-    value_rows = project(w_value)
-    gate_out = project(w_gate_out)
-    gate_in = project(w_gate_in)
-    conv_in = project(w_conv_in)
     bias = jnp.transpose(key_bias.astype(jnp.float32)) * LOG2E
     bias_high = lax.reduce_precision(bias, 8, 7)
     bias_low = bias - bias_high
     extra = jnp.stack([bias_high, bias_low], axis=1).reshape(2 * head_count, tok_rows)
     extra = jnp.pad(extra, ((0, -2 * head_count % 16), (0, 0))).astype(jnp.bfloat16)
-    keys = jnp.concatenate([key_cols, extra], axis=0)
+    queries, keys, value_rows, gate_out, gate_in, conv_in = project_all(
+        tokens,
+        norm_gain[None, :],
+        extra,
+        (w_query, w_key, w_value, w_gate_out, w_gate_in, w_conv_in),
+        lax.axis_size("tp"),
+    )
     attn_gain = lax.dynamic_slice_in_dim(mix_gain, tp_index * head_cols, head_cols)
     edge_rows = CONV_WIDTH - 1
     tail_rows = jnp.stack([gate_in[tok_rows - edge_rows :], conv_in[tok_rows - edge_rows :]])

time: 163 us -> 142 us (0.87)
  waiting for transfers between devices: 35.8 us -> 1.61 us
  Pallas kernels: 86.3 us -> 115 us
  between operations: 13.6 us -> 0.12 us
  local copies, waits for them, and re-layouts: 9.94 us -> 19.2 us
  matrix products: 8.7 us -> 0 us
  other arithmetic: 6.82 us -> 4 us
    all_gather x1 -> x0, waiting for transfers between devices: 35.1 us -> none  [per_device(): gathered = lax.all_gather(tokens, 'tp', axis=1, tiled=True)]
    pallas_call x0 -> x1, Pallas kernels: none -> 29.6 us  [project_all(): pl.pallas_call(functools.partial(project_kernel, tp), name='front', out_s...]
    dot_general x6 -> x0, matrix products: 8.7 us -> none  [the longest x5 7.37 us: project(): jnp.dot(normed, weight, preferred_element_type=jnp.float32)]
    unnamed x21 -> x19, local copies, waits for them, and re-layouts: 4.93 us -> 12.5 us
    reduce_sum x1 -> x0, other arithmetic: 3.23 us -> none  [per_device(): jnp.mean(tok_float * tok_float, axis=1, keepdims=True) + eps]
    convert_element_type x1 -> x0, other arithmetic: 1.66 us -> none  [per_device(): normed = (tok_float * row_scale * norm_gain).astype(jnp.bfloat16)]
  transfers between devices with their start and end apart: 2 -> 1, of which waited for: 1 -> 1; matrix products, arithmetic and copies ran while one was open for 4% -> 1% of each run, Pallas kernels for 0% -> 0%
where the time goes in v3:
time: 142 us; the launch traced here: 141 us
  Pallas kernels  115 us (81%)
  local copies, waits for them, and re-layouts  19.2 us (14%)
  other arithmetic  4 us (3%)
  waiting for transfers between devices  1.61 us (1%)
    pallas_call x1, Pallas kernels, attend(): pl.pallas_call(functools.partial(attend_kernel, n, wide, tp), name='atten...  85 us
    pallas_call x1, Pallas kernels, project_all(): pl.pallas_call(functools.partial(project_kernel, tp), name='front', out_s...  29.6 us
    unnamed x19, local copies, waits for them, and re-layouts  12.5 us
    mul x2, local copies, waits for them, and re-layouts, group_norm(): grouped * lax.rsqrt(jnp.mean(grouped * grouped, axis=-1, keepdims=True) +...  2.89 us
  transfers between devices with their start and end apart: 1, of which 1 were waited for; matrix products, arithmetic and copies ran while one was open for 1% of the time, Pallas kernels for 0%

profile of v3, /device:TPU:29, one launch (start us, length us, event | category | flops | bytes accessed | tf_op | source)
XLA Modules:
  0.0 140.9 jit_solution(9076178675255159818)
XLA Ops:
  0.0 0.7 fusion.8
  0.8 0.0 copy-start.2
  0.8 1.6 %copy-done.2 = bf16[4096,256]{1,0:T(8,128)(2,1)S(1)} copy-done((bf16[4096,256]{1,0:T(8,128)(2,1)S(1)}, bf16[4096,256]{1,0:T(8,128)(2,1)}, u32[]{:S(2)}) %copy-start.2) | copy-done | bytes 2097176
  2.3 0.0 copy-start.3
  2.3 1.6 %copy-done.3 = bf16[4096,256]{1,0:T(8,128)(2,1)S(1)} copy-done((bf16[4096,256]{1,0:T(8,128)(2,1)S(1)}, bf16[4096,256]{1,0:T(8,128)(2,1)}, u32[]{:S(2)}) %copy-start.3) | copy-done | bytes 2097176
  3.9 0.0 copy-start.4
  3.9 1.6 %copy-done.4 = bf16[4096,256]{1,0:T(8,128)(2,1)S(1)} copy-done((bf16[4096,256]{1,0:T(8,128)(2,1)S(1)}, bf16[4096,256]{1,0:T(8,128)(2,1)}, u32[]{:S(2)}) %copy-start.4) | copy-done | bytes 2097176
  5.5 0.0 copy-start.5
  5.5 1.6 %copy-done.5 = bf16[4096,256]{1,0:T(8,128)(2,1)S(1)} copy-done((bf16[4096,256]{1,0:T(8,128)(2,1)S(1)}, bf16[4096,256]{1,0:T(8,128)(2,1)}, u32[]{:S(2)}) %copy-start.5) | copy-done | bytes 2097176
  7.1 0.0 copy-start.6
  7.1 1.6 %copy-done.6 = bf16[4096,256]{1,0:T(8,128)(2,1)S(1)} copy-done((bf16[4096,256]{1,0:T(8,128)(2,1)S(1)}, bf16[4096,256]{1,0:T(8,128)(2,1)}, u32[]{:S(2)}) %copy-start.6) | copy-done | bytes 2097176
  8.7 0.0 copy-start.7
  8.7 1.2 copy-done.7
  9.9 0.0 copy-start.8
  9.9 0.7 copy-done.8
  10.7 29.6 %front.1 = (bf16[512,256]{1,0:T(8,128)(2,1)S(1)}, bf16[272,512]{1,0:T(8,128)(2,1)S(1)}, bf16[512,256]{1,0:T(8,128)(2,1)S(1)}, bf16[512,256]{1,0:T(8,128)(2,1)S(1...) custom-call(bf16[512,1024]{1,0:T(8,128)(2,1)S(1)} %copy-done.7, f32[1,4096]{1,0:T(1,128)S(1)} %bitcast.25, ...), custom_call_target="tpu_custom_call" | custom-call | tf_op jit(solution)/shard_map/front/pallas_call | solution.py:530
  40.3 1.3 collective-permute-start
  41.6 0.1 convert_multiply_fusion
  41.7 0.9 constant_dynamic-slice_fusion
  42.6 0.8 fusion.11
  43.4 1.6 %collective-permute-done = bf16[2,2,256]{2,1,0:T(2,128)(2,1)S(1)} collective-permute-done((bf16[2,2,256]{2,1,0:T(2,128)(2,1)S(1)}, bf16[2,2,256]{2,1,0:T(2,128)(2,1)S(1)}, u32[]{:S(2)}, u32[]{:S(2)}) %collective-permute-start) | collective-permute-done | bytes 2080 | tf_op jit(solution)/shard_map/ppermute | solution.py:25
  45.0 1.0 fusion.9
  46.0 0.0 copy-start
  46.0 2.2 %copy.16 = f32[512,256]{0,1:T(8,128)} copy(f32[512,256]{1,0:T(8,128)} %get-tuple-element.17) | data formatting | bytes 1048576 | tf_op jit(solution)/shard_map/mul | solution.py:553
  48.2 1.1 bitcast_reduce_fusion
  49.3 0.9 mul.100
  50.1 2.0 %copy.17 = f32[512,256]{1,0:T(8,128)} copy(f32[512,256]{0,1:T(8,128)} %bitcast.27) | data formatting | bytes 1048576 | tf_op jit(solution)/shard_map/mul | solution.py:553
  52.2 1.1 multiply_convert_fusion.conv_ref
  53.3 0.0 copy-done
  53.3 0.0 copy-start.1
  53.3 1.6 %copy-done.1 = bf16[256,4096]{1,0:T(8,128)(2,1)S(1)} copy-done((bf16[256,4096]{1,0:T(8,128)(2,1)S(1)}, bf16[256,4096]{1,0:T(8,128)(2,1)}, u32[]{:S(2)}) %copy-start.1) | copy-done | bytes 2097176
  54.9 85.0 %attend.1 = bf16[512,1024]{1,0:T(8,128)(2,1)S(1)} custom-call(bf16[512,256]{1,0:T(8,128)(2,1)S(1)} %get-tuple-element.11.q_ref, bf16[272,512]{1,0:T(8,128)(2,1)S(1)} %get-tuple-element.12.k_ref, bf16[512,256]{1,0:T(8,128)(2,1)S(1)} %get-tuple-element.13.v_ref, f32[1,256]{1,0:T(1,128)S(1)} %bitcast.26, bf16[512,256]{1,0:T(8,128)(2,1)S(1)} %multiply_convert_fusion.conv_ref, ...), custom_call_target="tpu_custom_call" | custom-call | tf_op jit(solution)/shard_map/attend/pallas_call | solution.py:383
  139.9 1.0 copy.19
  (8 shorter events, 0.1 us)
Async XLA Ops:
  0.8 1.6 %copy-start.2 = (bf16[4096,256]{1,0:T(8,128)(2,1)S(1)}, bf16[4096,256]{1,0:T(8,128)(2,1)}, u32[]{:S(2)}) copy-start(bf16[4096,256]{1,0:T(8,128)(2,1)} %refs_0_.1) | copy-start | bytes 6291460
  2.3 1.6 %copy-start.3 = (bf16[4096,256]{1,0:T(8,128)(2,1)S(1)}, bf16[4096,256]{1,0:T(8,128)(2,1)}, u32[]{:S(2)}) copy-start(bf16[4096,256]{1,0:T(8,128)(2,1)} %refs_1_.1) | copy-start | bytes 6291460
  3.9 1.6 %copy-start.4 = (bf16[4096,256]{1,0:T(8,128)(2,1)S(1)}, bf16[4096,256]{1,0:T(8,128)(2,1)}, u32[]{:S(2)}) copy-start(bf16[4096,256]{1,0:T(8,128)(2,1)} %refs_2_.1) | copy-start | bytes 6291460
  5.5 1.6 %copy-start.5 = (bf16[4096,256]{1,0:T(8,128)(2,1)S(1)}, bf16[4096,256]{1,0:T(8,128)(2,1)}, u32[]{:S(2)}) copy-start(bf16[4096,256]{1,0:T(8,128)(2,1)} %refs_3_.1) | copy-start | bytes 6291460
  7.1 1.6 %copy-start.6 = (bf16[4096,256]{1,0:T(8,128)(2,1)S(1)}, bf16[4096,256]{1,0:T(8,128)(2,1)}, u32[]{:S(2)}) copy-start(bf16[4096,256]{1,0:T(8,128)(2,1)} %refs_4_.1) | copy-start | bytes 6291460
  8.7 1.2 copy-start.7
  9.9 0.7 copy-start.8
  40.3 4.6 %collective-permute-start = (bf16[2,2,256]{2,1,0:T(2,128)(2,1)S(1)}, bf16[2,2,256]{2,1,0:T(2,128)(2,1)S(1)}, u32[]{:S(2)}, u32[]{:S(2)}) collective-permute-start(bf16[2,2,256]{2,1,0:T(2,128)(2,1)S(1)} %pad_maximum_fusion.2), channel_id=1, source_target_pairs={{0,4},{4,8},{8,12},{12,16},{16,20},{20,24},{24,28},{1,5},{5,9},{9,... | collective-permute-start | bytes 6152 | tf_op jit(solution)/shard_map/ppermute | solution.py:25
  46.0 7.3 %copy-start = (bf16[256,4096]{1,0:T(8,128)(2,1)S(1)}, bf16[256,4096]{1,0:T(8,128)(2,1)}, u32[]{:S(2)}) copy-start(bf16[256,4096]{1,0:T(8,128)(2,1)} %wattn_ref.1) | copy-start | bytes 6291460
  53.3 1.6 %copy-start.1 = (bf16[256,4096]{1,0:T(8,128)(2,1)S(1)}, bf16[256,4096]{1,0:T(8,128)(2,1)}, u32[]{:S(2)}) copy-start(bf16[256,4096]{1,0:T(8,128)(2,1)} %wconv_ref.1) | copy-start | bytes 6291460
